TPU v7x, 32 devices: a whole 2x2x4 slice. The times are simulated.
32 devices in a mesh: kv: 16 (over z, y, x), tp: 2 (over core).
Axes of the slice: x: 2, y: 2, z: 4, core: 2. Of those that a mesh axis runs over, the one named last changes fastest.
Arguments:
- tokens: bfloat16 [8, 2048, 2048], P(None, 'kv'), may hold values from -32 to 32, as said below
- w_query: bfloat16 [2048, 1024], P(None, 'tp'), may hold values from -0.125 to 0.125
- w_key: bfloat16 [2048, 512], P(None, 'tp'), may hold values from -0.125 to 0.125
- w_value: bfloat16 [2048, 512], P(None, 'tp'), may hold values from -0.125 to 0.125
- w_output: bfloat16 [1024, 2048], P(None, 'tp'), may hold values from -3 to 3
- chosen: int32 [8, 16, 32], P(None, 'kv'), may hold values from -1 to 15, as said below
- lengths: int32 [8], replicated, may hold values from 1 to 2048, 5632 in all
Outputs:
- mixed: bfloat16 [8, 2048, 2048], P(None, 'kv', 'tp')
Inputs may be any that keep to these rules, and one draw needn't show every extreme that they name: chosen[s, b] lists distinct blocks of sequence s, none above b; its first entry is b; entries after the named ones are -1. For b >= 1 and each c < b, at most 4 of the 8 lists chosen[:, b] name block c, and exactly 4 of them name block b - 1. lengths[s] is the number of live positions of sequence s; the largest is 2048. `tokens`: activations of order one; some rows may be much larger.
All inputs are finite; a program needn't handle non-finite values.
Results may differ from a plain program's by a relative error of at most 0.012.
The roundings to bfloat16 on the way count: a program that leaves them out, or rounds other values in their place, can miss the bound.
Values may be sent and summed in bfloat16 or wider, within the bound.
No kernel may reach another device: no remote copies, remote signals or barrier semaphores. Data moves between devices by JAX's collectives and lax.ppermute only.
A program may use at most 128 MiB of HBM per device.

v0:
```python
import jax
import jax.numpy as jnp
from jax import lax
from jax.sharding import PartitionSpec as P

HEADS = 16
KV_HEADS = 8
HEAD_DIM = 64
CAP = 4


def per_device(tokens, w_query, w_key, w_value, w_output, chosen, lengths):
    seq_count, block_len, model_width = tokens.shape
    flat_rows = tokens.reshape(seq_count * block_len, model_width)
    queries = jnp.dot(flat_rows, w_query, preferred_element_type=jnp.float32).astype(jnp.bfloat16)
    key_proj = jnp.dot(flat_rows, w_key, preferred_element_type=jnp.float32).astype(jnp.bfloat16)
    value_proj = jnp.dot(flat_rows, w_value, preferred_element_type=jnp.float32).astype(
        jnp.bfloat16
    )
    key_width = key_proj.shape[1]
    local_blocks = jnp.concatenate([key_proj, value_proj], axis=1).reshape(
        seq_count, block_len, 2 * key_width
    )
    shard_member = lax.axis_index("kv")
    kv_devices = lax.axis_size("kv")
    picked = chosen[:, 0, :]
    clipped = jnp.maximum(picked, 0)
    seq_index = jnp.arange(seq_count, dtype=jnp.int32)
    owners = jnp.arange(kv_devices, dtype=jnp.int32)
    wanted = (
        jnp.any(picked[:, :, None] == owners[None, None, :], axis=1)
        & (owners != shard_member)[None, :]
    )
    wanted = wanted.T
    ranked = jnp.cumsum(wanted.astype(jnp.int32), axis=1) - 1
    slot_hit = wanted[:, :, None] & (
        ranked[:, :, None] == jnp.arange(CAP, dtype=jnp.int32)[None, None, :]
    )
    request = jnp.sum(slot_hit.astype(jnp.int32) * (seq_index + 1)[None, :, None], axis=1) - 1
    incoming = lax.all_to_all(request, "kv", split_axis=0, concat_axis=0, tiled=True)
    outgoing = local_blocks[jnp.maximum(incoming, 0)]
    arrived = lax.all_to_all(outgoing, "kv", split_axis=0, concat_axis=0, tiled=True)
    key_lookup = jnp.concatenate(
        [local_blocks, arrived.reshape(kv_devices * CAP, block_len, 2 * key_width)], axis=0
    )
    rank_at = jnp.take_along_axis(ranked.T, clipped, axis=1)
    source = jnp.where(
        picked == shard_member, seq_index[:, None], seq_count + clipped * CAP + rank_at
    )
    group_size = HEADS // KV_HEADS
    local_kv_heads = key_width // HEAD_DIM
    query_pos = shard_member * block_len + jnp.arange(block_len, dtype=jnp.int32)
    score_scale = HEAD_DIM ** (-0.5)

    def attend(packed):
        query_rows, source_row, pick_row, length = packed
        fetched = key_lookup[source_row]
        slot_count = pick_row.shape[0]
        key_rows = fetched[:, :, :key_width].reshape(
            slot_count * block_len, local_kv_heads, HEAD_DIM
        )
        value_rows = fetched[:, :, key_width:].reshape(
            slot_count * block_len, local_kv_heads, HEAD_DIM
        )
        grouped = query_rows.reshape(block_len, local_kv_heads, group_size, HEAD_DIM)
        scores = (
            jnp.einsum("qkgd,nkd->kgqn", grouped, key_rows, preferred_element_type=jnp.float32)
            * score_scale
        )
        key_pos = (
            pick_row[:, None] * block_len + jnp.arange(block_len, dtype=jnp.int32)[None, :]
        ).reshape(-1)
        listed = jnp.repeat(pick_row >= 0, block_len)
        allowed = (
            listed[None, :] & (key_pos[None, :] <= query_pos[:, None]) & (key_pos[None, :] < length)
        )
        masked = jnp.where(allowed, scores, -1e30)
        row_max = jnp.max(masked, axis=-1, keepdims=True)
        exponent = jnp.exp(masked - row_max)
        weights = (exponent / jnp.sum(exponent, axis=-1, keepdims=True)).astype(jnp.bfloat16)
        mixed_heads = jnp.einsum(
            "kgqn,nkd->qkgd", weights, value_rows, preferred_element_type=jnp.float32
        )
        live_rows = (query_pos < length)[:, None, None, None]
        return jnp.where(live_rows, mixed_heads, 0.0).astype(jnp.bfloat16).reshape(block_len, -1)

    attended = lax.map(attend, (queries.reshape(seq_count, block_len, -1), source, picked, lengths))
    attended_rows = attended.reshape(seq_count * block_len, -1)
    summed = jnp.dot(
        lax.all_gather(attended_rows, "tp", axis=1, tiled=True),
        w_output,
        preferred_element_type=jnp.float32,
    )
    return summed.astype(jnp.bfloat16).reshape(seq_count, block_len, -1)


def solution(mesh):
    return jax.shard_map(
        per_device,
        mesh=mesh,
        in_specs=(
            P(None, "kv", None),
            P(None, "tp"),
            P(None, "tp"),
            P(None, "tp"),
            P(None, "tp"),
            P(None, "kv", None),
            P(),
        ),
        out_specs=P(None, "kv", "tp"),
        check_vma=False,
    )
```

profile of v0, /device:TPU:0, one launch (start us, length us, event | category | flops | bytes accessed | tf_op | source)
XLA Modules:
  0.0 852.4 jit_solution(16968193628493152081)
XLA Ops:
  8.4 8.3 all-to-all-start
  45.0 147.7 %all-to-all-done.1 = bf16[16,4,128,512]{3,2,1,0:T(8,128)(2,1)} async-done(((bf16[16,4,128,512]{3,2,1,0:T(8,128)(2,1)}), bf16[16,4,128,512]{3,2,1,0:T(8,128)(2,1)}, u32[]{:S(2)}, u32[]{:S(2)}) %all-to-all-start.1) | async-done | bytes 8388640 | tf_op jit(solution)/shard_map/all_to_all | solution.py:42
  200.5 595.3 %while.11 = (s32[]{:T(128)}, bf16[8,128,512]{2,1,0:T(8,128)(2,1)}, s32[8]{0:T(128)S(1)}, s32[8,32]{1,0:T(8,128)S(1)}, bf16[72,128,512]{2,1,0:T(8,128)(2,1)}, /*i...) while((s32[]{:T(128)}, bf16[8,128,512]{2,1,0:T(8,128)(2,1)}, ...), condition=%wide.region_6.7_spmd.clone, body=%wide.region_3.0_spmd.clone.sunk | while | flops 1109018112 | bytes 107281480 | solution.py:87
  226.3 9.7 %fusion.49 = f32[4,4096,128,2]{2,1,3,0:T(8,128)} fusion(bf16[128,4,2,64]{0,3,2,1:T(8,128)(2,1)S(1)} %bitcast.106, bf16[4096,4,64,1]{0,2,1,3:T(8,128)(2,1)} %reshape.219), kind=kOutput, calls=%fused_computation.13.clone.1 | convolution fusion | flops 536870912 | bytes 19005440 | tf_op jit(solution)/shard_map/while/body/eval_jaxpr/qkgd,nkd->kgqn/dot_general | solution.py:67
  236.0 20.9 %fusion.50 = (f32[4,2,128]{2,1,0:T(2,128)S(1)}, f32[4,2,128,4096]{2,3,1,0:T(8,128)}) fusion(f32[4,4096,128,2]{2,1,3,0:T(8,128)} %fusion.49, pred[128,4096]{0,1:T(8,128)(4,1)S(1)} %and_and_fusion.2), kind=kOutput, calls=%fused_computation.60.clone.1 | output fusion | flops 25169920 | bytes 34082816 | tf_op jit(solution)/shard_map/while/body/eval_jaxpr/sub | solution.py:79
  266.2 8.0 fusion.51
  300.7 9.7 %fusion.49 = f32[4,4096,128,2]{2,1,3,0:T(8,128)} fusion(bf16[128,4,2,64]{0,3,2,1:T(8,128)(2,1)S(1)} %bitcast.106, bf16[4096,4,64,1]{0,2,1,3:T(8,128)(2,1)} %reshape.219), kind=kOutput, calls=%fused_computation.13.clone.1 | convolution fusion | flops 536870912 | bytes 19005440 | tf_op jit(solution)/shard_map/while/body/eval_jaxpr/qkgd,nkd->kgqn/dot_general | solution.py:67
  310.4 20.9 %fusion.50 = (f32[4,2,128]{2,1,0:T(2,128)S(1)}, f32[4,2,128,4096]{2,3,1,0:T(8,128)}) fusion(f32[4,4096,128,2]{2,1,3,0:T(8,128)} %fusion.49, pred[128,4096]{0,1:T(8,128)(4,1)S(1)} %and_and_fusion.2), kind=kOutput, calls=%fused_computation.60.clone.1 | output fusion | flops 25169920 | bytes 34082816 | tf_op jit(solution)/shard_map/while/body/eval_jaxpr/sub | solution.py:79
  340.6 8.0 fusion.51
  375.1 9.7 %fusion.49 = f32[4,4096,128,2]{2,1,3,0:T(8,128)} fusion(bf16[128,4,2,64]{0,3,2,1:T(8,128)(2,1)S(1)} %bitcast.106, bf16[4096,4,64,1]{0,2,1,3:T(8,128)(2,1)} %reshape.219), kind=kOutput, calls=%fused_computation.13.clone.1 | convolution fusion | flops 536870912 | bytes 19005440 | tf_op jit(solution)/shard_map/while/body/eval_jaxpr/qkgd,nkd->kgqn/dot_general | solution.py:67
  384.8 20.9 %fusion.50 = (f32[4,2,128]{2,1,0:T(2,128)S(1)}, f32[4,2,128,4096]{2,3,1,0:T(8,128)}) fusion(f32[4,4096,128,2]{2,1,3,0:T(8,128)} %fusion.49, pred[128,4096]{0,1:T(8,128)(4,1)S(1)} %and_and_fusion.2), kind=kOutput, calls=%fused_computation.60.clone.1 | output fusion | flops 25169920 | bytes 34082816 | tf_op jit(solution)/shard_map/while/body/eval_jaxpr/sub | solution.py:79
  415.0 8.0 fusion.51
  449.5 9.7 %fusion.49 = f32[4,4096,128,2]{2,1,3,0:T(8,128)} fusion(bf16[128,4,2,64]{0,3,2,1:T(8,128)(2,1)S(1)} %bitcast.106, bf16[4096,4,64,1]{0,2,1,3:T(8,128)(2,1)} %reshape.219), kind=kOutput, calls=%fused_computation.13.clone.1 | convolution fusion | flops 536870912 | bytes 19005440 | tf_op jit(solution)/shard_map/while/body/eval_jaxpr/qkgd,nkd->kgqn/dot_general | solution.py:67
  459.2 20.9 %fusion.50 = (f32[4,2,128]{2,1,0:T(2,128)S(1)}, f32[4,2,128,4096]{2,3,1,0:T(8,128)}) fusion(f32[4,4096,128,2]{2,1,3,0:T(8,128)} %fusion.49, pred[128,4096]{0,1:T(8,128)(4,1)S(1)} %and_and_fusion.2), kind=kOutput, calls=%fused_computation.60.clone.1 | output fusion | flops 25169920 | bytes 34082816 | tf_op jit(solution)/shard_map/while/body/eval_jaxpr/sub | solution.py:79
  489.4 8.0 fusion.51
  523.9 9.7 %fusion.49 = f32[4,4096,128,2]{2,1,3,0:T(8,128)} fusion(bf16[128,4,2,64]{0,3,2,1:T(8,128)(2,1)S(1)} %bitcast.106, bf16[4096,4,64,1]{0,2,1,3:T(8,128)(2,1)} %reshape.219), kind=kOutput, calls=%fused_computation.13.clone.1 | convolution fusion | flops 536870912 | bytes 19005440 | tf_op jit(solution)/shard_map/while/body/eval_jaxpr/qkgd,nkd->kgqn/dot_general | solution.py:67
  533.6 20.9 %fusion.50 = (f32[4,2,128]{2,1,0:T(2,128)S(1)}, f32[4,2,128,4096]{2,3,1,0:T(8,128)}) fusion(f32[4,4096,128,2]{2,1,3,0:T(8,128)} %fusion.49, pred[128,4096]{0,1:T(8,128)(4,1)S(1)} %and_and_fusion.2), kind=kOutput, calls=%fused_computation.60.clone.1 | output fusion | flops 25169920 | bytes 34082816 | tf_op jit(solution)/shard_map/while/body/eval_jaxpr/sub | solution.py:79
  598.3 9.7 %fusion.49 = f32[4,4096,128,2]{2,1,3,0:T(8,128)} fusion(bf16[128,4,2,64]{0,3,2,1:T(8,128)(2,1)S(1)} %bitcast.106, bf16[4096,4,64,1]{0,2,1,3:T(8,128)(2,1)} %reshape.219), kind=kOutput, calls=%fused_computation.13.clone.1 | convolution fusion | flops 536870912 | bytes 19005440 | tf_op jit(solution)/shard_map/while/body/eval_jaxpr/qkgd,nkd->kgqn/dot_general | solution.py:67
  608.0 20.9 %fusion.50 = (f32[4,2,128]{2,1,0:T(2,128)S(1)}, f32[4,2,128,4096]{2,3,1,0:T(8,128)}) fusion(f32[4,4096,128,2]{2,1,3,0:T(8,128)} %fusion.49, pred[128,4096]{0,1:T(8,128)(4,1)S(1)} %and_and_fusion.2), kind=kOutput, calls=%fused_computation.60.clone.1 | output fusion | flops 25169920 | bytes 34082816 | tf_op jit(solution)/shard_map/while/body/eval_jaxpr/sub | solution.py:79
  672.7 9.7 %fusion.49 = f32[4,4096,128,2]{2,1,3,0:T(8,128)} fusion(bf16[128,4,2,64]{0,3,2,1:T(8,128)(2,1)S(1)} %bitcast.106, bf16[4096,4,64,1]{0,2,1,3:T(8,128)(2,1)} %reshape.219), kind=kOutput, calls=%fused_computation.13.clone.1 | convolution fusion | flops 536870912 | bytes 19005440 | tf_op jit(solution)/shard_map/while/body/eval_jaxpr/qkgd,nkd->kgqn/dot_general | solution.py:67
  682.4 20.9 %fusion.50 = (f32[4,2,128]{2,1,0:T(2,128)S(1)}, f32[4,2,128,4096]{2,3,1,0:T(8,128)}) fusion(f32[4,4096,128,2]{2,1,3,0:T(8,128)} %fusion.49, pred[128,4096]{0,1:T(8,128)(4,1)S(1)} %and_and_fusion.2), kind=kOutput, calls=%fused_computation.60.clone.1 | output fusion | flops 25169920 | bytes 34082816 | tf_op jit(solution)/shard_map/while/body/eval_jaxpr/sub | solution.py:79
  747.1 9.7 %fusion.49 = f32[4,4096,128,2]{2,1,3,0:T(8,128)} fusion(bf16[128,4,2,64]{0,3,2,1:T(8,128)(2,1)S(1)} %bitcast.106, bf16[4096,4,64,1]{0,2,1,3:T(8,128)(2,1)} %reshape.219), kind=kOutput, calls=%fused_computation.13.clone.1 | convolution fusion | flops 536870912 | bytes 19005440 | tf_op jit(solution)/shard_map/while/body/eval_jaxpr/qkgd,nkd->kgqn/dot_general | solution.py:67
  756.8 20.9 %fusion.50 = (f32[4,2,128]{2,1,0:T(2,128)S(1)}, f32[4,2,128,4096]{2,3,1,0:T(8,128)}) fusion(f32[4,4096,128,2]{2,1,3,0:T(8,128)} %fusion.49, pred[128,4096]{0,1:T(8,128)(4,1)S(1)} %and_and_fusion.2), kind=kOutput, calls=%fused_computation.60.clone.1 | output fusion | flops 25169920 | bytes 34082816 | tf_op jit(solution)/shard_map/while/body/eval_jaxpr/sub | solution.py:79
  795.8 44.5 %all-gather.2.cloned.1.call-done = bf16[1024,1024]{1,0:T(8,128)(2,1)} async-done(((bf16[1024,512]{1,0:T(8,128)(2,1)}), bf16[1024,1024]{1,0:T(8,128)(2,1)}) %all-gather.2.cloned.1.call-update) | async-done | bytes 2097168 | tf_op jit(solution)/shard_map/all_gather | solution.py:90
  (213 shorter events, 361.4 us)
Async XLA Ops:
  6.5 833.8 %copy-start = (bf16[1024,1024]{1,0:T(8,128)(2,1)S(1)}, bf16[1024,1024]{1,0:T(8,128)(2,1)}, u32[]{:S(2)}) copy-start(bf16[1024,1024]{1,0:T(8,128)(2,1)} %param.13) | copy-start | bytes 6291460
  8.4 16.3 %all-to-all-start = ((s32[16,1,4]{2,1,0:T(1,128)}), s32[16,1,4]{2,1,0:T(1,128)S(1)}, u32[]{:S(2)}, u32[]{:S(2)}) async-start(s32[16,1,4]{2,1,0:T(1,128)} %copy.40), calls=%async_computation | async-start | bytes 16384 | tf_op jit(solution)/shard_map/all_to_all | solution.py:40
  16.8 4.0 copy-start.2
  16.8 4.0 copy-start.3
  30.2 6.9 copy-start.1
  30.3 162.5 %all-to-all-start.1 = ((bf16[16,4,128,512]{3,2,1,0:T(8,128)(2,1)}), bf16[16,4,128,512]{3,2,1,0:T(8,128)(2,1)}, u32[]{:S(2)}, u32[]{:S(2)}) async-start(bf16[16,4,128,512]{3,2,1,0:T(8,128)(2,1)} %bitcast.105), calls=%async_computation.1 | async-start | bytes 16777216 | tf_op jit(solution)/shard_map/all_to_all | solution.py:42
  37.1 803.2 %all-gather.2.cloned.1.call-start = ((), (), s32[]{:S(2)}) async-start(), calls=%async_computation.2 | async-start | bytes 3145728 | tf_op jit(solution)/shard_map/all_gather | solution.py:90
  192.7 7.8 copy-start.4
Sparse Core Ops, SparseCore 0:
  795.9 44.3 all-gather.1
where the time goes:
time: 856 us; the launch traced here: 852 us
  local copies, waits for them, and re-layouts  258 us (30%)
  other arithmetic  215 us (25%)
  waiting for transfers between devices  192 us (22%)
  matrix products  158 us (18%)
  starting transfers between devices  15.3 us (2%)
  between operations  13.5 us (2%)
    sub x8, other arithmetic, attend(): exponent = jnp.exp(masked - row_max)  167 us
    all_to_all x1, waiting for transfers between devices, per_device(): lax.all_to_all(outgoing, 'kv', split_axis=0, concat_axis=0, tiled=True)  148 us
    dot_general x8, matrix products, attend(): jnp.einsum('qkgd,nkd->kgqn', grouped, key_rows, preferred_element_type=jn...  77.5 us
    slice x16, local copies, waits for them, and re-layouts, attend(): fetched[:, :, key_width:]  74.6 us
    dot_general x8, matrix products, attend(): jnp.einsum('kgqn,nkd->qkgd', weights, value_rows, preferred_element_type=...  63.9 us
    gather x8, local copies, waits for them, and re-layouts, attend(): fetched = key_lookup[source_row]  51.4 us
    all_gather x1, waiting for transfers between devices, per_device(): lax.all_gather(attended_rows, 'tp', axis=1, tiled=True)  44.5 us
    slice x8, local copies, waits for them, and re-layouts, attend(): fetched[:, :, :key_width]  36.4 us
  transfers between devices with their start and end apart: 3, of which 2 were waited for; matrix products, arithmetic and copies ran while one was open for 2% of the time, Pallas kernels for 0%

commit v1 on v0

--- a/solution.py
+++ b/solution.py
@@ -1,15 +1,22 @@
+import functools
+
 import jax
 import jax.numpy as jnp
 from jax import lax
+from jax.experimental import pallas as pl
+from jax.experimental.pallas import tpu as pltpu
 from jax.sharding import PartitionSpec as P
 
 HEADS = 16
 KV_HEADS = 8
 HEAD_DIM = 64
 CAP = 4
-
-
-def per_device(tokens, w_query, w_key, w_value, w_output, chosen, lengths):
+META_ROWS = 16
+LANES = 128
+GROUP = 4
+
+
+def per_device_general(tokens, w_query, w_key, w_value, w_output, chosen, lengths):
     seq_count, block_len, model_width = tokens.shape
     flat_rows = tokens.reshape(seq_count * block_len, model_width)
     queries = jnp.dot(flat_rows, w_query, preferred_element_type=jnp.float32).astype(jnp.bfloat16)
@@ -94,19 +101,267 @@
     return summed.astype(jnp.bfloat16).reshape(seq_count, block_len, -1)
 
 
+def project_kernel(order_ref, *refs, slots, kv_local):
+    token_refs = refs[:slots]
+    wq_ref, wk_ref, wv_ref, meta_ref, out_ref = refs[slots:]
+    plane = pl.program_id(0)
+    blk = token_refs[0].shape[1]
+    rows = jnp.concatenate([t[0] for t in token_refs], axis=0)
+    q = jnp.dot(rows, wq_ref[...], preferred_element_type=jnp.float32).astype(jnp.bfloat16)
+    k = jnp.dot(rows, wk_ref[...], preferred_element_type=jnp.float32).astype(jnp.bfloat16)
+    v = jnp.dot(rows, wv_ref[...], preferred_element_type=jnp.float32).astype(jnp.bfloat16)
+    for h in range(kv_local):
+        dest = plane * kv_local + h
+        q_h = q[:, h * LANES:(h + 1) * LANES]
+        kv_h = jnp.concatenate(
+            [k[:, h * HEAD_DIM:(h + 1) * HEAD_DIM], v[:, h * HEAD_DIM:(h + 1) * HEAD_DIM]], axis=1
+        )
+        for j in range(slots):
+            base = j * 2 * blk
+            out_ref[dest, base:base + blk, :] = q_h[j * blk:(j + 1) * blk]
+            out_ref[dest, base + blk:base + 2 * blk, :] = kv_h[j * blk:(j + 1) * blk]
+        out_ref[dest, slots * 2 * blk:, :] = meta_ref[0]
+
+
+def project(tokens, w_query, w_key, w_value, meta, order, planes, slots, kv_local):
+    seq_count, blk, width = tokens.shape
+    rows = slots * 2 * blk + META_ROWS
+
+    def token_map(j):
+        return lambda p, order_ref: (order_ref[j * planes + p], 0, 0)
+
+    whole = lambda a: pl.BlockSpec(a.shape, lambda p, o: (0,) * a.ndim)
+    dests = planes * kv_local
+    return pl.pallas_call(
+        functools.partial(project_kernel, slots=slots, kv_local=kv_local),
+        grid_spec=pltpu.PrefetchScalarGridSpec(
+            num_scalar_prefetch=1,
+            grid=(planes,),
+            in_specs=[pl.BlockSpec((1, blk, width), token_map(j)) for j in range(slots)]
+            + [whole(w_query), whole(w_key), whole(w_value)]
+            + [pl.BlockSpec((1, META_ROWS, LANES), lambda p, o: (p, 0, 0))],
+            out_specs=pl.BlockSpec((dests, rows, LANES), lambda p, o: (0, 0, 0)),
+        ),
+        out_shape=jax.ShapeDtypeStruct((dests, rows, LANES), jnp.bfloat16),
+        compiler_params=pltpu.CompilerParams(vmem_limit_bytes=48 << 20),
+        cost_estimate=pl.CostEstimate(
+            flops=2 * seq_count * blk * width * 2 * kv_local * LANES,
+            transcendentals=0,
+            bytes_accessed=2 * (tokens.size + w_query.size * 2 + dests * rows * LANES),
+        ),
+        name="project",
+    )(order, *([tokens] * slots), w_query, w_key, w_value, meta)
+
+
+def attend_kernel(lens_ref, list_ref, in_ref, out_ref, *, slots, blocks, blk, stride):
+    lane = lax.broadcasted_iota(jnp.int32, (blk, LANES), 1)
+    low = lane < HEAD_DIM
+    scale = HEAD_DIM ** -0.5
+
+    def one(j, b, length):
+        base = pl.multiple_of(j * 2 * blk, 2 * blk)
+        meta = (b * slots + j) * LANES
+        q = in_ref[b, pl.ds(base, blk), :]
+        rolled = jnp.where(low, pltpu.roll(q.astype(jnp.float32), HEAD_DIM, 1), 0.0)
+        q0 = jnp.where(low, q.astype(jnp.float32), 0.0)
+        q2 = (jnp.concatenate([q0, rolled], axis=0) * scale).astype(jnp.bfloat16)
+        count = list_ref[meta + stride]
+
+        def body(groups):
+            total = groups * GROUP
+            kvs = []
+            for t in range(total):
+                c = jnp.maximum(list_ref[meta + t], 0)
+                kvs.append(in_ref[c, pl.ds(base + blk, blk), :])
+            kv = jnp.concatenate(kvs, axis=0)
+            s = lax.dot_general(
+                q2, kv, (((1,), (1,)), ((), ())), preferred_element_type=jnp.float32
+            )
+            row = lax.broadcasted_iota(jnp.int32, (2 * blk, blk), 0) % blk
+            col = lax.broadcasted_iota(jnp.int32, (2 * blk, blk), 1)
+            parts = []
+            for t in range(total):
+                part = s[:, t * blk:(t + 1) * blk]
+                if t == 0:
+                    part = jnp.where(col <= row, part, -1e30)
+                elif t > total - GROUP:
+                    part = jnp.where(t < count, part, -1e30)
+                parts.append(part)
+            peak = parts[0]
+            for part in parts[1:]:
+                peak = jnp.maximum(peak, part)
+            m = jnp.max(peak, axis=1, keepdims=True)
+            exps = [jnp.exp(part - m) for part in parts]
+            acc = exps[0]
+            for e in exps[1:]:
+                acc = acc + e
+            denom = jnp.sum(acc, axis=1, keepdims=True)
+            p = jnp.concatenate([e.astype(jnp.bfloat16) for e in exps], axis=1)
+            o = jnp.dot(p, kv, preferred_element_type=jnp.float32) / denom
+            o = jnp.where(low, pltpu.roll(o[:blk], HEAD_DIM, 1), o[blk:])
+            pos = b * blk + lax.broadcasted_iota(jnp.int32, (blk, LANES), 0)
+            out_ref[b, pl.ds(pl.multiple_of(j * blk, blk), blk), :] = jnp.where(
+                pos < length, o, 0.0
+            ).astype(jnp.bfloat16)
+
+        for groups in range(1, -(-blocks // GROUP) + 1):
+            @pl.when((count > (groups - 1) * GROUP) & (count <= groups * GROUP))
+            def _():
+                body(groups)
+
+    for j in range(slots):
+        length = lens_ref[j]
+
+        @pl.loop(0, blocks)
+        def _(b):
+            @pl.when(b * blk < length)
+            def _():
+                one(j, b, length)
+
+            @pl.when(b * blk >= length)
+            def _():
+                out_ref[b, j * blk:(j + 1) * blk, :] = jnp.zeros((blk, LANES), jnp.bfloat16)
+
+
+def attend(arrived, lens, lists, slots, blk, stride):
+    blocks = arrived.shape[0]
+    return pl.pallas_call(
+        functools.partial(attend_kernel, slots=slots, blocks=blocks, blk=blk, stride=stride),
+        grid_spec=pltpu.PrefetchScalarGridSpec(
+            num_scalar_prefetch=2,
+            grid=(1,),
+            in_specs=[pl.BlockSpec(arrived.shape, lambda i, a, b: (0, 0, 0))],
+            out_specs=pl.BlockSpec((blocks, slots * blk, LANES), lambda i, a, b: (0, 0, 0)),
+        ),
+        out_shape=jax.ShapeDtypeStruct((blocks, slots * blk, LANES), jnp.bfloat16),
+        compiler_params=pltpu.CompilerParams(vmem_limit_bytes=48 << 20),
+        cost_estimate=pl.CostEstimate(
+            flops=4 * 2 * blk * blk * LANES * 100, transcendentals=0, bytes_accessed=3 << 20
+        ),
+        name="attend",
+    )(lens, lists, arrived)
+
+
+def output_kernel(order_ref, own_ref, other_ref, w_ref, out_ref, *, slots, planes, kv_local):
+    plane = pl.program_id(0)
+    blk = out_ref.shape[1]
+    half = kv_local * LANES
+    side = order_ref[slots * planes]
+
+    def rows(ref):
+        return jnp.concatenate(
+            [
+                jnp.concatenate([ref[h, j * blk:(j + 1) * blk, :] for h in range(kv_local)], axis=1)
+                for j in range(slots)
+            ],
+            axis=0,
+        )
+
+    own_at = pl.multiple_of(side * half, half)
+    other_at = pl.multiple_of((1 - side) * half, half)
+    o = jnp.dot(rows(own_ref), w_ref[pl.ds(own_at, half), :], preferred_element_type=jnp.float32)
+    o = o + jnp.dot(
+        rows(other_ref), w_ref[pl.ds(other_at, half), :], preferred_element_type=jnp.float32
+    )
+    o = o.astype(jnp.bfloat16)
+    for j in range(slots):
+        out_ref[order_ref[j * planes + plane]] = o[j * blk:(j + 1) * blk]
+
+
+def output_projection(own, other, w_output, order, planes, slots, kv_local, blk):
+    seq_count = planes * slots
+    width = w_output.shape[1]
+    return pl.pallas_call(
+        functools.partial(output_kernel, slots=slots, planes=planes, kv_local=kv_local),
+        grid_spec=pltpu.PrefetchScalarGridSpec(
+            num_scalar_prefetch=1,
+            grid=(planes,),
+            in_specs=[
+                pl.BlockSpec((kv_local, slots * blk, LANES), lambda p, o: (p, 0, 0)),
+                pl.BlockSpec((kv_local, slots * blk, LANES), lambda p, o: (p, 0, 0)),
+                pl.BlockSpec(w_output.shape, lambda p, o: (0, 0)),
+            ],
+            out_specs=pl.BlockSpec((seq_count, blk, width), lambda p, o: (0, 0, 0)),
+        ),
+        out_shape=jax.ShapeDtypeStruct((seq_count, blk, width), jnp.bfloat16),
+        compiler_params=pltpu.CompilerParams(vmem_limit_bytes=48 << 20),
+        cost_estimate=pl.CostEstimate(
+            flops=2 * seq_count * blk * w_output.size, transcendentals=0, bytes_accessed=6 << 20
+        ),
+        name="output_projection",
+    )(order, own, other, w_output)
+
+
+def per_device(tokens, w_query, w_key, w_value, w_output, chosen, lengths):
+    seq_count, blk, _ = tokens.shape
+    kv_devices = lax.axis_size("kv")
+    kv_local = w_key.shape[1] // HEAD_DIM
+    planes = kv_devices // kv_local
+    slots = seq_count // planes
+    select = chosen.shape[2]
+    seq_ids = jnp.arange(seq_count, dtype=jnp.int32)
+    longer = (lengths[None, :] > lengths[:, None]) | (
+        (lengths[None, :] == lengths[:, None]) & (seq_ids[None, :] < seq_ids[:, None])
+    )
+    rank = jnp.sum(longer.astype(jnp.int32), axis=1)
+    turn, step = rank // planes, rank % planes
+    place = turn * planes + jnp.where(turn % 2 == 0, step, planes - 1 - step)
+    order = jnp.sum(jnp.where(place[None, :] == seq_ids[:, None], seq_ids[None, :], 0), axis=1)
+
+    picked = chosen[:, 0, :]
+    count = jnp.sum((picked >= 0).astype(jnp.int32), axis=1, keepdims=True)
+    meta = jnp.concatenate([picked, count], axis=1).astype(jnp.bfloat16)
+    meta = jnp.pad(meta, ((0, 0), (0, LANES - select - 1)))
+    hit = (order[:, None] == seq_ids[None, :]).astype(jnp.bfloat16)
+    meta = jnp.dot(hit, meta, preferred_element_type=jnp.float32).astype(jnp.bfloat16)
+    meta = meta.reshape(slots, planes, LANES).transpose(1, 0, 2)
+    meta = jnp.pad(meta, ((0, 0), (0, META_ROWS - slots), (0, 0)))
+
+    payload = project(
+        tokens, w_query, w_key, w_value, meta, order, planes, slots, kv_local
+    )
+    arrived = lax.all_to_all(payload, "kv", split_axis=0, concat_axis=0, tiled=True)
+    lists = arrived[:, slots * 2 * blk:slots * 2 * blk + slots, :].astype(jnp.int32).reshape(-1)
+    my_plane = lax.axis_index("kv") // kv_local
+    mine = jnp.arange(slots, dtype=jnp.int32) * planes + my_plane
+    my_seqs = jnp.sum(jnp.where(mine[:, None] == seq_ids[None, :], order[None, :], 0), axis=1)
+    lens = jnp.sum(jnp.where(my_seqs[:, None] == seq_ids[None, :], lengths[None, :], 0), axis=1)
+    attended = attend(arrived, lens, lists, slots, blk, select)
+    own = lax.all_to_all(attended, "kv", split_axis=0, concat_axis=0, tiled=True)
+    other = lax.ppermute(own, "tp", [(0, 1), (1, 0)])
+    order_side = jnp.concatenate([order, lax.axis_index("tp").astype(jnp.int32)[None]])
+    return output_projection(own, other, w_output, order_side, planes, slots, kv_local, blk)
+
+
+def fits(mesh, tokens, w_key, chosen):
+    kv_devices, tp_devices = mesh.shape["kv"], mesh.shape["tp"]
+    kv_local = w_key.shape[1] // tp_devices // HEAD_DIM
+    if HEADS // KV_HEADS * HEAD_DIM != LANES or 2 * HEAD_DIM != LANES or tp_devices != 2:
+        return False
+    if kv_local == 0 or kv_devices % kv_local or kv_devices > 16 or chosen.shape[2] >= LANES:
+        return False
+    planes = kv_devices // kv_local
+    blk = tokens.shape[1] // kv_devices
+    return tokens.shape[0] % planes == 0 and tokens.shape[0] // planes <= META_ROWS and blk == LANES
+
+
 def solution(mesh):
-    return jax.shard_map(
-        per_device,
-        mesh=mesh,
-        in_specs=(
-            P(None, "kv", None),
-            P(None, "tp"),
-            P(None, "tp"),
-            P(None, "tp"),
-            P(None, "tp"),
-            P(None, "kv", None),
-            P(),
-        ),
-        out_specs=P(None, "kv", "tp"),
-        check_vma=False,
-    )
+    def run(tokens, w_query, w_key, w_value, w_output, chosen, lengths):
+        body = per_device if fits(mesh, tokens, w_key, chosen) else per_device_general
+        return jax.shard_map(
+            body,
+            mesh=mesh,
+            in_specs=(
+                P(None, "kv", None),
+                P(None, "tp"),
+                P(None, "tp"),
+                P(None, "tp"),
+                P(None, "tp"),
+                P(None, "kv", None),
+                P(),
+            ),
+            out_specs=P(None, "kv", "tp"),
+            check_vma=False,
+        )(tokens, w_query, w_key, w_value, w_output, chosen, lengths)
+
+    return run

time: 856 us -> 122 us (0.14)
  local copies, waits for them, and re-layouts: 258 us -> 5.75 us
  other arithmetic: 215 us -> 2.51 us
  matrix products: 158 us -> 0.19 us
  waiting for transfers between devices: 192 us -> 46.3 us
  blocking collectives: 0 us -> 32.1 us
  Pallas kernels: 0 us -> 27.3 us
  between operations: 13.5 us -> 0.08 us
    sub x10 -> x0, other arithmetic: 167 us -> none  [the longest x8 167 us: attend(): exponent = jnp.exp(masked - row_max)]
    dot_general x20 -> x1, matrix products: 158 us -> 0.19 us  [per_device(): jnp.dot(hit, meta, preferred_element_type=jnp.float32).astype(jnp.bfloat16)]
    slice x24 -> x1, local copies, waits for them, and re-layouts: 111 us -> 0.01 us  [per_device(): arrived[:, slots * 2 * blk:slots * 2 * blk + slots, :].astype(jnp.int32)]
    all_to_all x2 -> x1, waiting for transfers between devices: 148 us -> 43.8 us  [per_device(): lax.all_to_all(payload, 'kv', split_axis=0, concat_axis=0, tiled=True)]
    reshape x17 -> x1, local copies, waits for them, and re-layouts: 68.1 us -> 0.01 us  [per_device(): meta = meta.reshape(slots, planes, LANES).transpose(1, 0, 2)]
    gather x12 -> x0, local copies, waits for them, and re-layouts: 58.4 us -> none  [the longest x8 51.4 us: attend(): fetched = key_lookup[source_row]]
    all_gather x1 -> x0, waiting for transfers between devices: 44.5 us -> none  [per_device(): lax.all_gather(attended_rows, 'tp', axis=1, tiled=True)]
    all_to_all x0 -> x1, blocking collectives: none -> 32.1 us  [per_device(): lax.all_to_all(attended, 'kv', split_axis=0, concat_axis=0, tiled=True)]
  transfers between devices with their start and end apart: 3 -> 2, of which waited for: 2 -> 2; matrix products, arithmetic and copies ran while one was open for 2% -> 0% of each run, Pallas kernels for 0% -> 0%
where the time goes in v1:
time: 122 us; the launch traced here: 123 us
  waiting for transfers between devices  46.3 us (38%)
  blocking collectives  32.1 us (26%)
  Pallas kernels  27.3 us (22%)
  starting transfers between devices  8.48 us (7%)
  local copies, waits for them, and re-layouts  5.75 us (5%)
  other arithmetic  2.51 us (2%)
    all_to_all x1, waiting for transfers between devices, per_device(): lax.all_to_all(payload, 'kv', split_axis=0, concat_axis=0, tiled=True)  43.8 us
    all_to_all x1, blocking collectives, per_device(): lax.all_to_all(attended, 'kv', split_axis=0, concat_axis=0, tiled=True)  32.1 us
    pallas_call x1, Pallas kernels, attend(): pl.pallas_call(functools.partial(attend_kernel, slots=slots, blocks=block...  14.1 us
    pallas_call x1, Pallas kernels, project(): pl.pallas_call(functools.partial(project_kernel, slots=slots, kv_local=kv...  8.47 us
    all_to_all x1, starting transfers between devices, per_device(): lax.all_to_all(payload, 'kv', split_axis=0, concat_axis=0, tiled=True)  8.47 us
    unnamed x11, local copies, waits for them, and re-layouts  5.63 us
    pallas_call x1, Pallas kernels, output_projection(): pl.pallas_call(functools.partial(output_kernel, slots=slots, planes=plane...  4.74 us
    ppermute x1, waiting for transfers between devices, per_device(): other = lax.ppermute(own, 'tp', [(0, 1), (1, 0)])  2.58 us
  transfers between devices with their start and end apart: 2, of which 2 were waited for; matrix products, arithmetic and copies ran while one was open for 0% of the time, Pallas kernels for 0%

profile of v1, /device:TPU:0, one launch (start us, length us, event | category | flops | bytes accessed | tf_op | source)
XLA Modules:
  0.0 122.8 jit_solution(16959663357119569027)
XLA Ops:
  0.0 0.9 convert_reduce_fusion
  0.9 0.1 select_reduce_fusion.order_ref
  1.1 1.0 fusion.20
  2.1 0.1 copy.11
  2.2 0.2 convolution_convert_fusion
  2.4 1.6 %copy-done = bf16[2048,512]{1,0:T(8,128)(2,1)S(1)} copy-done((bf16[2048,512]{1,0:T(8,128)(2,1)S(1)}, bf16[2048,512]{1,0:T(8,128)(2,1)}, u32[]{:S(2)}) %copy-start) | copy-done | bytes 2097176
  4.0 0.0 copy-start.2
  4.0 1.2 copy-done.2
  5.2 0.0 copy-start.3
  5.2 1.2 copy-done.3
  6.4 8.5 %project.1 = bf16[16,528,128]{2,1,0:T(8,128)(2,1)} custom-call(s32[8]{0:T(128)S(1)} %select_reduce_fusion.order_ref, bf16[8,128,2048]{2,1,0:T(8,128)(2,1)} %refs_1_.1, bf16[8,128,2048]{2,1,0:T(8,128)(2,1)} %refs_1_.1, bf16[2048,512]{1,0:T(8,128)(2,1)S(1)} %copy-done, bf16[2048,256]{1,0:T(8,128)(2,1)S(1)} %copy-done.2, bf16[2048,256]{1,0:T(8,128)(2,1)S(1)} %copy-done.3, ...), custom_call_target="tpu_custom_call" | custom-call | flops 4294967296 | bytes 10551296 | tf_op jit(solution)/shard_map/project/pallas_call | solution.py:135
  14.9 0.0 copy-start.4
  14.9 8.5 %all-to-all-start = ((bf16[16,528,128]{2,1,0:T(8,128)(2,1)}), bf16[16,528,128]{2,1,0:T(8,128)(2,1)S(1)}, u32[]{:S(2)}, u32[]{:S(2)}) async-start(bf16[16,528,128]{2,1,0:T(8,128)(2,1)} %project.1), calls=%async_computation | async-start | bytes 4325376 | tf_op jit(solution)/shard_map/all_to_all | solution.py:323
  23.4 0.2 fusion.12
  23.6 0.0 copy-done.4
  23.6 0.2 fusion.13.lens_ref
  23.8 43.8 %all-to-all-done.in_ref = bf16[16,528,128]{2,1,0:T(8,128)(2,1)S(1)} async-done(((bf16[16,528,128]{2,1,0:T(8,128)(2,1)}), bf16[16,528,128]{2,1,0:T(8,128)(2,1)S(1)}, u32[]{:S(2)}, u32[]{:S(2)}) %all-to-all-start) | async-done | bytes 2162720 | tf_op jit(solution)/shard_map/all_to_all | solution.py:323
  67.6 14.1 %attend.1 = bf16[16,256,128]{2,1,0:T(8,128)(2,1)S(1)} custom-call(s32[2]{0:T(128)S(1)} %fusion.13.lens_ref, s32[4096]{0:T(1024)S(1)} %convert.11.list_ref, bf16[16,528,128]{2,1,0:T(8,128)(2,1)S(1)} %all-to-all-done.in_ref), custom_call_target="tpu_custom_call" | custom-call | flops 1677721600 | bytes 3145728 | tf_op jit(solution)/shard_map/attend/pallas_call | solution.py:228
  81.6 32.1 %all_to_all.10.own_ref = bf16[16,256,128]{2,1,0:T(8,128)(2,1)S(1)} all-to-all(bf16[16,256,128]{2,1,0:T(8,128)(2,1)S(1)} %attend.1), channel_id=1, replica_groups=mesh['kv'=16,'tp'=2] {'kv'}, dimensions={0} | all-to-all | bytes 2097152 | tf_op jit(solution)/shard_map/all_to_all | solution.py:330
  113.8 0.0 collective-permute-start
  113.8 0.1 pad_add_fusion.order_ref
  113.8 2.6 %collective-permute-done.other_ref = bf16[16,256,128]{2,1,0:T(8,128)(2,1)S(1)} collective-permute-done((bf16[16,256,128]{2,1,0:T(8,128)(2,1)S(1)}, bf16[16,256,128]{2,1,0:T(8,128)(2,1)S(1)}, u32[]{:S(2)}, u32[]{:S(2)}) %collective-permute-start) | collective-permute-done | bytes 1048608 | tf_op jit(solution)/shard_map/ppermute | solution.py:331
  116.4 1.6 %copy-done.1 = bf16[1024,1024]{1,0:T(8,128)(2,1)S(1)} copy-done((bf16[1024,1024]{1,0:T(8,128)(2,1)S(1)}, bf16[1024,1024]{1,0:T(8,128)(2,1)}, u32[]{:S(2)}) %copy-start.1) | copy-done | bytes 2097176
  118.0 4.7 %output_projection.1 = bf16[8,128,1024]{2,1,0:T(8,128)(2,1)} custom-call(s32[9]{0:T(128)S(1)} %pad_add_fusion.order_ref, bf16[16,256,128]{2,1,0:T(8,128)(2,1)S(1)} %all_to_all.10.own_ref, bf16[16,256,128]{2,1,0:T(8,128)(2,1)S(1)} %collective-permute-done.other_ref, bf16[1024,1024]{1,0:T(8,128)(2,1)S(1)} %copy-done.1), custom_call_target="tpu_custom_call" | custom-call | flops 2147483648 | bytes 6291456 | tf_op jit(solution)/shard_map/output_projection/pallas_call | solution.py:274
  (10 shorter events, 0.1 us)
Async XLA Ops:
  2.4 1.6 %copy-start = (bf16[2048,512]{1,0:T(8,128)(2,1)S(1)}, bf16[2048,512]{1,0:T(8,128)(2,1)}, u32[]{:S(2)}) copy-start(bf16[2048,512]{1,0:T(8,128)(2,1)} %refs_2_.1) | copy-start | bytes 6291460
  4.0 1.2 copy-start.2
  5.2 1.2 copy-start.3
  14.9 8.7 %copy-start.4 = (s32[8]{0:T(128)S(1)}, s32[8]{0:T(128)}, u32[]{:S(2)}) copy-start(s32[8]{0:T(128)} %param.13) | copy-start | bytes 100
  14.9 52.6 %all-to-all-start = ((bf16[16,528,128]{2,1,0:T(8,128)(2,1)}), bf16[16,528,128]{2,1,0:T(8,128)(2,1)S(1)}, u32[]{:S(2)}, u32[]{:S(2)}) async-start(bf16[16,528,128]{2,1,0:T(8,128)(2,1)} %project.1), calls=%async_computation | async-start | bytes 4325376 | tf_op jit(solution)/shard_map/all_to_all | solution.py:323
  113.8 2.7 %collective-permute-start = (bf16[16,256,128]{2,1,0:T(8,128)(2,1)S(1)}, bf16[16,256,128]{2,1,0:T(8,128)(2,1)S(1)}, u32[]{:S(2)}, u32[]{:S(2)}) collective-permute-start(bf16[16,256,128]{2,1,0:T(8,128)(2,1)S(1)} %all_to_all.10.own_ref), channel_id=1, source_target_pairs={{0,1},{1,0},{2,3},{3,2},{4,5},{5,4},{6,7},{7,6},{8,9},{9,8},{10,11... | collective-permute-start | bytes 3145736 | tf_op jit(solution)/shard_map/ppermute | solution.py:331
  116.4 1.6 %copy-start.1 = (bf16[1024,1024]{1,0:T(8,128)(2,1)S(1)}, bf16[1024,1024]{1,0:T(8,128)(2,1)}, u32[]{:S(2)}) copy-start(bf16[1024,1024]{1,0:T(8,128)(2,1)} %w_ref.1) | copy-start | bytes 6291460

commit v2 on v0

--- a/solution.py
+++ b/solution.py
@@ -1,15 +1,24 @@
+import functools
+
 import jax
 import jax.numpy as jnp
 from jax import lax
+from jax.experimental import pallas as pl
+from jax.experimental.pallas import tpu as pltpu
 from jax.sharding import PartitionSpec as P
 
 HEADS = 16
 KV_HEADS = 8
 HEAD_DIM = 64
 CAP = 4
-
-
-def per_device(tokens, w_query, w_key, w_value, w_output, chosen, lengths):
+META_ROWS = 16
+LANES = 128
+GROUP = 4
+VMEM_MOST = 63 << 20
+HBM = pltpu.HBM
+
+
+def per_device_general(tokens, w_query, w_key, w_value, w_output, chosen, lengths):
     seq_count, block_len, model_width = tokens.shape
     flat_rows = tokens.reshape(seq_count * block_len, model_width)
     queries = jnp.dot(flat_rows, w_query, preferred_element_type=jnp.float32).astype(jnp.bfloat16)
@@ -94,19 +103,417 @@
     return summed.astype(jnp.bfloat16).reshape(seq_count, block_len, -1)
 
 
+def order_by_length(lengths_ref, order_ref, seq_count):
+    for s in range(seq_count):
+        rank = jnp.int32(0)
+        for t in range(seq_count):
+            if t < s:
+                ahead = lengths_ref[t] >= lengths_ref[s]
+            elif t > s:
+                ahead = lengths_ref[t] > lengths_ref[s]
+            else:
+                continue
+            rank = rank + jnp.where(ahead, 1, 0)
+        order_ref[rank] = s
+
+
+def project_kernel(
+    lengths_ref, chosen_ref, tokens_ref, wq_ref, wk_ref, wv_ref, out_ref,
+    order_ref, meta_ref, rows_ref, wq_buf, wk_buf, wv_buf, row_sems, w_sems,
+    *, ranks, slots, kv_local, select,
+):
+    seq_count = chosen_ref.shape[0]
+    blk = tokens_ref.shape[1]
+    loads = [
+        pltpu.make_async_copy(wq_ref, wq_buf, w_sems.at[0]),
+        pltpu.make_async_copy(wk_ref, wk_buf, w_sems.at[1]),
+        pltpu.make_async_copy(wv_ref, wv_buf, w_sems.at[2]),
+    ]
+    order_by_length(lengths_ref, order_ref, seq_count)
+    fetch = [
+        pltpu.make_async_copy(
+            tokens_ref.at[order_ref[rank]], rows_ref.at[pl.ds(i * blk, blk)], row_sems.at[i]
+        )
+        for i, rank in enumerate(ranks)
+    ]
+    for f in fetch[:2]:
+        f.start()
+    for load in loads:
+        load.start()
+    for f in fetch[2:]:
+        f.start()
+    meta_ref[...] = jnp.zeros(meta_ref.shape, jnp.float32)
+    for s in range(seq_count):
+        meta_ref[s:s + 1, :select] = chosen_ref[s].astype(jnp.float32)
+    lane = lax.broadcasted_iota(jnp.int32, meta_ref.shape, 1)
+    named = meta_ref[...]
+    count = jnp.sum(jnp.where((lane < select) & (named >= 0), 1.0, 0.0), axis=1, keepdims=True)
+    meta_ref[...] = jnp.where(lane == select, count, named)
+    tile_row = lax.broadcasted_iota(jnp.int32, (META_ROWS, LANES), 0)
+    planes = len(ranks) // slots
+    for p in range(planes):
+        tile = jnp.zeros((META_ROWS, LANES), jnp.float32)
+        for j in range(slots):
+            row = meta_ref[pl.ds(order_ref[ranks[p * slots + j]], 1), :]
+            tile = jnp.where(tile_row == j, row, tile)
+        tile = tile.astype(jnp.bfloat16)
+        for h in range(kv_local):
+            out_ref[p * kv_local + h, slots * 2 * blk:, :] = tile
+    for load in loads:
+        load.wait()
+    for first in range(0, len(ranks), 2):
+        fetch[first].wait()
+        fetch[first + 1].wait()
+        rows = rows_ref[first * blk:(first + 2) * blk, :]
+        q = jnp.dot(rows, wq_buf[...], preferred_element_type=jnp.float32).astype(jnp.bfloat16)
+        k = jnp.dot(rows, wk_buf[...], preferred_element_type=jnp.float32).astype(jnp.bfloat16)
+        v = jnp.dot(rows, wv_buf[...], preferred_element_type=jnp.float32).astype(jnp.bfloat16)
+        for h in range(kv_local):
+            q_h = q[:, h * LANES:(h + 1) * LANES]
+            kv_h = jnp.concatenate(
+                [k[:, h * HEAD_DIM:(h + 1) * HEAD_DIM], v[:, h * HEAD_DIM:(h + 1) * HEAD_DIM]],
+                axis=1,
+            )
+            for i in range(2):
+                p, j = divmod(first + i, slots)
+                base = j * 2 * blk
+                out_ref[p * kv_local + h, base:base + blk, :] = q_h[i * blk:(i + 1) * blk]
+                out_ref[p * kv_local + h, base + blk:base + 2 * blk, :] = kv_h[i * blk:(i + 1) * blk]
+
+
+def project(tokens, w_query, w_key, w_value, chosen, lengths, ranks, slots, kv_local):
+    seq_count, blk, width = tokens.shape
+    dests = len(ranks) // slots * kv_local
+    rows = slots * 2 * blk + META_ROWS
+    hbm = pl.BlockSpec(memory_space=HBM)
+    return pl.pallas_call(
+        functools.partial(
+            project_kernel, ranks=ranks, slots=slots, kv_local=kv_local, select=chosen.shape[2]
+        ),
+        in_specs=[
+            pl.BlockSpec(memory_space=pltpu.SMEM),
+            pl.BlockSpec(memory_space=pltpu.VMEM),
+            hbm, hbm, hbm, hbm,
+        ],
+        out_specs=pl.BlockSpec(memory_space=pltpu.VMEM),
+        out_shape=jax.ShapeDtypeStruct((dests, rows, LANES), jnp.bfloat16),
+        scratch_shapes=[
+            pltpu.SMEM((seq_count,), jnp.int32),
+            pltpu.VMEM((seq_count, LANES), jnp.float32),
+            pltpu.VMEM((len(ranks) * blk, width), jnp.bfloat16),
+            pltpu.VMEM(w_query.shape, jnp.bfloat16),
+            pltpu.VMEM(w_key.shape, jnp.bfloat16),
+            pltpu.VMEM(w_value.shape, jnp.bfloat16),
+            pltpu.SemaphoreType.DMA((len(ranks),)),
+            pltpu.SemaphoreType.DMA((3,)),
+        ],
+        compiler_params=pltpu.CompilerParams(vmem_limit_bytes=VMEM_MOST),
+        cost_estimate=pl.CostEstimate(
+            flops=2 * len(ranks) * blk * width * 2 * kv_local * LANES,
+            transcendentals=0,
+            bytes_accessed=2 * (len(ranks) * blk * width + w_query.size * 2 + dests * rows * LANES),
+        ),
+        name="project",
+    )(lengths, chosen, tokens, w_query, w_key, w_value)
+
+
+def attend_kernel(
+    lengths_ref, where_ref, list_ref, far_ref, *refs, slots, split, planes, blocks, blk, stride,
+):
+    parts = slots // split
+    arrived, near, (out_ref, order_ref, q_buf, kv_buf, sems) = refs[:parts], refs[parts:-5], refs[-5:]
+    plane, start = where_ref[0], where_ref[1]
+    copies = []
+    for j in range(slots):
+        part, base = arrived[j // split], j % split * 2 * blk
+        copies.append((part.at[:, pl.ds(base, blk), :], q_buf.at[j]))
+        copies.append((part.at[:, pl.ds(base + blk, blk), :], kv_buf.at[j, pl.ds(start, blocks)]))
+    for j, ref in enumerate((far_ref,) + near):
+        copies.append((ref, kv_buf.at[j, pl.ds(blocks - start, blocks)]))
+    copies = [pltpu.make_async_copy(a, b, sems.at[i]) for i, (a, b) in enumerate(copies)]
+    for copy in copies:
+        copy.start()
+    order_by_length(lengths_ref, order_ref, lengths_ref.shape[0])
+    lane = lax.broadcasted_iota(jnp.int32, (blk, LANES), 1)
+    low = lane < HEAD_DIM
+    scale = HEAD_DIM ** -0.5
+    for copy in copies:
+        copy.wait()
+
+    def list_at(j, b):
+        return ((j // split * blocks + b) * split + j % split) * LANES
+
+    def head_rows(j, b):
+        q = q_buf[j, b].astype(jnp.float32)
+        q1 = jnp.where(low, pltpu.roll(q, HEAD_DIM, 1), 0.0)
+        q0 = jnp.where(low, q, 0.0)
+        return (jnp.concatenate([q0, q1], axis=0) * scale).astype(jnp.bfloat16)
+
+    def body(j, b, length, groups):
+        meta = list_at(j, b)
+        count = list_ref[meta + stride]
+        q2 = head_rows(j, b)
+        total = groups * GROUP
+        kvs = []
+        for t in range(total):
+            c = jnp.maximum(list_ref[meta + t], 0)
+            kvs.append(kv_buf[j, c])
+        kv = jnp.concatenate(kvs, axis=0)
+        s = lax.dot_general(q2, kv, (((1,), (1,)), ((), ())), preferred_element_type=jnp.float32)
+        row = lax.broadcasted_iota(jnp.int32, (2 * blk, blk), 0) % blk
+        col = lax.broadcasted_iota(jnp.int32, (2 * blk, blk), 1)
+        parts = []
+        for t in range(total):
+            part = s[:, t * blk:(t + 1) * blk]
+            if t == 0:
+                part = jnp.where(col <= row, part, -1e30)
+            else:
+                part = jnp.where(t < count, part, -1e30)
+            parts.append(part)
+        peak = parts[0]
+        for part in parts[1:]:
+            peak = jnp.maximum(peak, part)
+        m = jnp.max(peak, axis=1, keepdims=True)
+        exps = [jnp.exp(part - m) for part in parts]
+        acc = exps[0]
+        for e in exps[1:]:
+            acc = acc + e
+        denom = jnp.sum(acc, axis=1, keepdims=True)
+        p = jnp.concatenate([e.astype(jnp.bfloat16) for e in exps], axis=1)
+        o = jnp.dot(p, kv, preferred_element_type=jnp.float32) / denom
+        o = jnp.where(low, pltpu.roll(o[:blk], HEAD_DIM, 1), o[blk:])
+        pos = (start + b) * blk + lax.broadcasted_iota(jnp.int32, (blk, LANES), 0)
+        out_ref[b, pl.ds(pl.multiple_of(j * blk, blk), blk), :] = jnp.where(
+            pos < length, o, 0.0
+        ).astype(jnp.bfloat16)
+
+    @pl.loop(0, slots * blocks // 2)
+    def _(step):
+        j, b = step // (blocks // 2), step % (blocks // 2) * 2
+        rank = j * planes + jnp.where(j % 2 == 0, plane, planes - 1 - plane)
+        length = lengths_ref[order_ref[rank]]
+        live = (start + b) * blk < length
+
+        @pl.when(live)
+        def _():
+            need = jnp.maximum(
+                list_ref[list_at(j, b) + stride], list_ref[list_at(j, b + 1) + stride]
+            )
+            for groups in range(1, -(-2 * blocks // GROUP) + 1):
+                @pl.when((need > (groups - 1) * GROUP) & (need <= groups * GROUP))
+                def _():
+                    body(j, b, length, groups)
+                    body(j, b + 1, length, groups)
+
+        @pl.when(jnp.logical_not(live))
+        def _():
+            zero = jnp.zeros((blk, LANES), jnp.bfloat16)
+            out_ref[b, pl.ds(pl.multiple_of(j * blk, blk), blk), :] = zero
+            out_ref[b + 1, pl.ds(pl.multiple_of(j * blk, blk), blk), :] = zero
+
+
+def attend(arrived, from_half, lengths, where, lists, split, planes, blk, stride):
+    blocks = arrived[0].shape[0]
+    slots = split * len(arrived)
+    smem = pl.BlockSpec(memory_space=pltpu.SMEM)
+    vmem = pl.BlockSpec(memory_space=pltpu.VMEM)
+    anywhere = pl.BlockSpec(memory_space=pl.ANY)
+    far, *near = from_half
+    return pl.pallas_call(
+        functools.partial(
+            attend_kernel, slots=slots, split=split, planes=planes, blocks=blocks, blk=blk,
+            stride=stride,
+        ),
+        in_specs=[smem, smem, smem] + [anywhere] * (len(from_half) + len(arrived)),
+        out_specs=vmem,
+        out_shape=jax.ShapeDtypeStruct((blocks, slots * blk, LANES), jnp.bfloat16),
+        scratch_shapes=[
+            pltpu.SMEM(lengths.shape, jnp.int32),
+            pltpu.VMEM((slots, blocks, blk, LANES), jnp.bfloat16),
+            pltpu.VMEM((slots, 2 * blocks, blk, LANES), jnp.bfloat16),
+            pltpu.SemaphoreType.DMA((2 * slots + len(from_half),)),
+        ],
+        compiler_params=pltpu.CompilerParams(vmem_limit_bytes=40 << 20),
+        cost_estimate=pl.CostEstimate(
+            flops=4 * 2 * blk * blk * LANES * blocks * blocks // 2 * slots,
+            transcendentals=0,
+            bytes_accessed=3 << 20,
+        ),
+        name="attend",
+    )(lengths, where, lists, far, *arrived, *near)
+
+
+def output_kernel(
+    lengths_ref, side_ref, own_ref, other_ref, w_ref, out_ref,
+    order_ref, w_buf, rows_buf, sem, out_sems, *, planes, kv_local,
+):
+    seq_count, blk = out_ref.shape[0], out_ref.shape[1]
+    load = pltpu.make_async_copy(w_ref, w_buf, sem)
+    load.start()
+    order_by_length(lengths_ref, order_ref, seq_count)
+    half = kv_local * LANES
+    own_at = pl.multiple_of(side_ref[0] * half, half)
+    other_at = pl.multiple_of((1 - side_ref[0]) * half, half)
+
+    def rows(ref, rank):
+        p, j = place(rank, planes)
+        return jnp.concatenate(
+            [ref[p * kv_local + h, j * blk:(j + 1) * blk, :] for h in range(kv_local)], axis=1
+        )
+
+    load.wait()
+    stores = []
+    for rank in range(0, seq_count, 2):
+        mine = jnp.concatenate([rows(own_ref, rank), rows(own_ref, rank + 1)], axis=0)
+        theirs = jnp.concatenate([rows(other_ref, rank), rows(other_ref, rank + 1)], axis=0)
+        o = jnp.dot(mine, w_buf[pl.ds(own_at, half), :], preferred_element_type=jnp.float32)
+        o = o + jnp.dot(
+            theirs, w_buf[pl.ds(other_at, half), :], preferred_element_type=jnp.float32
+        )
+        rows_buf[rank:rank + 2] = o.astype(jnp.bfloat16).reshape(2, blk, -1)
+        for r in (rank, rank + 1):
+            store = pltpu.make_async_copy(
+                rows_buf.at[r], out_ref.at[order_ref[r]], out_sems.at[r]
+            )
+            store.start()
+            stores.append(store)
+    for store in stores:
+        store.wait()
+
+
+def output_projection(own, other, w_output, lengths, side, planes, kv_local, blk):
+    seq_count = lengths.shape[0]
+    width = w_output.shape[1]
+    smem = pl.BlockSpec(memory_space=pltpu.SMEM)
+    vmem = pl.BlockSpec(memory_space=pltpu.VMEM)
+    hbm = pl.BlockSpec(memory_space=HBM)
+    return pl.pallas_call(
+        functools.partial(output_kernel, planes=planes, kv_local=kv_local),
+        in_specs=[smem, smem, vmem, vmem, hbm],
+        out_specs=hbm,
+        out_shape=jax.ShapeDtypeStruct((seq_count, blk, width), jnp.bfloat16),
+        scratch_shapes=[
+            pltpu.SMEM((seq_count,), jnp.int32),
+            pltpu.VMEM(w_output.shape, jnp.bfloat16),
+            pltpu.VMEM((seq_count, blk, width), jnp.bfloat16),
+            pltpu.SemaphoreType.DMA,
+            pltpu.SemaphoreType.DMA((seq_count,)),
+        ],
+        compiler_params=pltpu.CompilerParams(vmem_limit_bytes=40 << 20),
+        cost_estimate=pl.CostEstimate(
+            flops=2 * seq_count * blk * w_output.size, transcendentals=0, bytes_accessed=6 << 20
+        ),
+        name="output_projection",
+    )(lengths, side, own, other, w_output)
+
+
+def place(rank, planes):
+    j, step = divmod(rank, planes)
+    return (step if j % 2 == 0 else planes - 1 - step), j
+
+
+def per_device(tokens, w_query, w_key, w_value, w_output, chosen, lengths):
+    seq_count, blk, _ = tokens.shape
+    kv_devices = lax.axis_size("kv")
+    kv_local = w_key.shape[1] // HEAD_DIM
+    half = kv_devices // 2
+    planes = half // kv_local
+    slots = seq_count // planes
+    split = slots // 2
+    select = chosen.shape[2]
+    ranks = {place(rank, planes): rank for rank in range(seq_count)}
+    groups = [
+        tuple(ranks[p, part * split + j] for p in range(planes) for j in range(split))
+        for part in range(2)
+    ]
+    halves = [list(range(half)), list(range(half, kv_devices))]
+
+    def exchange(x):
+        return lax.all_to_all(
+            x, "kv", split_axis=0, concat_axis=0, tiled=True, axis_index_groups=halves
+        )
+
+    def lists_of(arrived):
+        at = split * 2 * blk
+        return arrived[:, at:at + split, :].astype(jnp.int32)
+
+    def to_second_half(x):
+        return lax.ppermute(x, "kv", [(i, i + half) for i in range(half)])
+
+    here = lax.axis_index("kv").astype(jnp.int32)
+    where = jnp.stack([here % half // kv_local, here // half * half])
+    sent_a = project(tokens, w_query, w_key, w_value, chosen, lengths, groups[0], split, kv_local)
+    arrived_a = exchange(sent_a)
+    later, _ = lax.optimization_barrier((lengths, sent_a))
+    sent_b = project(tokens, w_query, w_key, w_value, chosen, later, groups[1], split, kv_local)
+    from_half = []
+    for j in range(split):
+        kv = arrived_a[:, (2 * j + 1) * blk:(2 * j + 2) * blk, :]
+        if j == 0:
+            from_half.append(to_second_half(kv))
+        else:
+            longer = jnp.sum((lengths > half * blk).astype(jnp.int32)) > j * planes
+            from_half.append(lax.cond(longer, to_second_half, lambda x: x, kv))
+    arrived_b = exchange(sent_b)
+    lists = jnp.concatenate([lists_of(arrived_a), lists_of(arrived_b)]).reshape(-1)
+    attended = attend(
+        [arrived_a, arrived_b], from_half, lengths, where, lists, split, planes, blk, select
+    )
+    own = exchange(attended)
+    other = lax.ppermute(own, "tp", [(0, 1), (1, 0)])
+    side = lax.axis_index("tp").astype(jnp.int32)[None]
+    return output_projection(own, other, w_output, lengths, side, planes, kv_local, blk)
+
+
+def fits(mesh, tokens, w_key, chosen):
+    seq_count, seq_len = tokens.shape[0], tokens.shape[1]
+    kv_devices, tp_devices = mesh.shape["kv"], mesh.shape["tp"]
+    kv_local = w_key.shape[1] // tp_devices // HEAD_DIM
+    if HEADS // KV_HEADS * HEAD_DIM != LANES or 2 * HEAD_DIM != LANES or tp_devices != 2:
+        return False
+    if kv_local == 0 or kv_devices % (4 * kv_local) or kv_devices > 16 or chosen.shape[2] >= LANES:
+        return False
+    planes = kv_devices // 2 // kv_local
+    if seq_len // kv_devices != LANES or seq_count % (2 * planes) or seq_count % 4:
+        return False
+    split = seq_count // planes // 2
+    fits_half = (seq_count - 1) * seq_len // 4 // (split * planes) <= seq_len // 2
+    return split <= META_ROWS and planes * split % 2 == 0 and fits_half
+
+
+def fits(mesh, tokens, w_key, chosen):
+    seq_count, seq_len = tokens.shape[0], tokens.shape[1]
+    kv_devices, tp_devices = mesh.shape["kv"], mesh.shape["tp"]
+    kv_local = w_key.shape[1] // tp_devices // HEAD_DIM
+    if HEADS // KV_HEADS * HEAD_DIM != LANES or 2 * HEAD_DIM != LANES or tp_devices != 2:
+        return False
+    if kv_local == 0 or kv_devices % (4 * kv_local) or kv_devices > 16 or chosen.shape[2] >= LANES:
+        return False
+    planes = kv_devices // kv_local
+    if seq_len // kv_devices != LANES or seq_count <= planes or seq_count % 2 or planes % 2:
+        return False
+    slots, odd = divmod(seq_count - planes, planes // 2)
+    fits_half = (seq_count - 1) * seq_len // 4 // planes <= seq_len // 2
+    return odd == 0 and slots <= META_ROWS and (planes // 2 * slots) % 2 == 0 and fits_half
+
+
 def solution(mesh):
-    return jax.shard_map(
-        per_device,
-        mesh=mesh,
-        in_specs=(
-            P(None, "kv", None),
-            P(None, "tp"),
-            P(None, "tp"),
-            P(None, "tp"),
-            P(None, "tp"),
-            P(None, "kv", None),
-            P(),
-        ),
-        out_specs=P(None, "kv", "tp"),
-        check_vma=False,
-    )
+    def run(tokens, w_query, w_key, w_value, w_output, chosen, lengths):
+        body = per_device if fits(mesh, tokens, w_key, chosen) else per_device_general
+        return jax.shard_map(
+            body,
+            mesh=mesh,
+            in_specs=(
+                P(None, "kv", None),
+                P(None, "tp"),
+                P(None, "tp"),
+                P(None, "tp"),
+                P(None, "tp"),
+                P(None, "kv", None),
+                P(),
+            ),
+            out_specs=P(None, "kv", "tp"),
+            check_vma=False,
+        )(tokens, w_query, w_key, w_value, w_output, chosen, lengths)
+
+    return run

time: 856 us -> 86.3 us (0.10)
  local copies, waits for them, and re-layouts: 258 us -> 1.81 us
  other arithmetic: 215 us -> 0.72 us
  waiting for transfers between devices: 192 us -> 20.4 us
  matrix products: 158 us -> 0 us
  Pallas kernels: 0 us -> 29.8 us
  blocking collectives: 0 us -> 17.9 us
  between operations: 13.5 us -> 0.67 us
    sub x10 -> x0, other arithmetic: 167 us -> none  [the longest x8 167 us: attend(): exponent = jnp.exp(masked - row_max)]
    dot_general x20 -> x0, matrix products: 158 us -> none  [the longest x8 77.5 us: attend(): jnp.einsum('qkgd,nkd->kgqn', grouped, key_rows, preferred_element_type=jn...]
    all_to_all x2, waiting for transfers between devices: 148 us -> 15.4 us  [exchange(): lax.all_to_all(x, 'kv', split_axis=0, concat_axis=0, tiled=True, axis_ind...]
    slice x24 -> x3, local copies, waits for them, and re-layouts: 111 us -> 1.8 us  [the longest x1 1.07 us: per_device(): kv = arrived_a[:, (2 * j + 1) * blk:(2 * j + 2) * blk, :]]
    reshape x17 -> x0, local copies, waits for them, and re-layouts: 68.1 us -> none  [the longest x8 33.4 us: attend(): fetched[:, :, :key_width]]
    gather x12 -> x0, local copies, waits for them, and re-layouts: 58.4 us -> none  [the longest x8 51.4 us: attend(): fetched = key_lookup[source_row]]
    all_gather x1 -> x0, waiting for transfers between devices: 44.5 us -> none  [per_device(): lax.all_gather(attended_rows, 'tp', axis=1, tiled=True)]
    pallas_call x0 -> x4, Pallas kernels: none -> 29.8 us  [the longest x2 14.2 us: project(): pl.pallas_call(functools.partial(project_kernel, ranks=ranks, slots=slots...]
  transfers between devices with their start and end apart: 3 -> 4, of which waited for: 2 -> 4; matrix products, arithmetic and copies ran while one was open for 2% -> 3% of each run, Pallas kernels for 0% -> 8%
where the time goes in v2:
time: 86.3 us; the launch traced here: 85.6 us
  Pallas kernels  29.8 us (35%)
  waiting for transfers between devices  20.4 us (24%)
  blocking collectives  17.9 us (21%)
  starting transfers between devices  14.3 us (17%)
  local copies, waits for them, and re-layouts  1.81 us (2%)
    all_to_all x1, blocking collectives, exchange(): lax.all_to_all(x, 'kv', split_axis=0, concat_axis=0, tiled=True, axis_ind...  17.9 us
    all_to_all x2, waiting for transfers between devices, exchange(): lax.all_to_all(x, 'kv', split_axis=0, concat_axis=0, tiled=True, axis_ind...  15.4 us
    pallas_call x2, Pallas kernels, project(): pl.pallas_call(functools.partial(project_kernel, ranks=ranks, slots=slots...  14.2 us
    pallas_call x1, Pallas kernels, attend(): pl.pallas_call(functools.partial(attend_kernel, slots=slots, split=split,...  10.9 us
    all_to_all x2, starting transfers between devices, exchange(): lax.all_to_all(x, 'kv', split_axis=0, concat_axis=0, tiled=True, axis_ind...  9.78 us
    pallas_call x1, Pallas kernels, output_projection(): pl.pallas_call(functools.partial(output_kernel, planes=planes, kv_local=k...  4.65 us
    ppermute x1, starting transfers between devices, to_second_half(): return lax.ppermute(x, 'kv', [(i, i + half) for i in range(half)])  4.51 us
    ppermute x1, waiting for transfers between devices, per_device(): other = lax.ppermute(own, 'tp', [(0, 1), (1, 0)])  2.79 us
  transfers between devices with their start and end apart: 4, of which 4 were waited for; matrix products, arithmetic and copies ran while one was open for 3% of the time, Pallas kernels for 8%

profile of v2, /device:TPU:0, one launch (start us, length us, event | category | flops | bytes accessed | tf_op | source)
XLA Modules:
  0.0 85.6 jit_solution(18006096724895743163)
XLA Ops:
  0.0 7.1 %project.2 = bf16[8,528,128]{2,1,0:T(8,128)(2,1)} custom-call(s32[8]{0:T(128)} %lengths_ref.6, s32[8,1,32]{2,1,0:T(1,128)} %chosen_ref.3, bf16[8,128,2048]{2,1,0:T(8,128)(2,1)} %tokens_ref.3, bf16[2048,512]{1,0:T(8,128)(2,1)} %wq_ref.3, bf16[2048,256]{1,0:T(8,128)(2,1)} %wk_ref.3, bf16[2048,256]{1,0:T(8,128)(2,1)} %wv_ref.3), custom_call_target="tpu_custom_call" | custom-call | flops 2147483648 | bytes 7372800 | tf_op jit(solution)/shard_map/project/pallas_call | solution.py:189
  7.2 6.2 %all-to-all-start = ((bf16[8,528,128]{2,1,0:T(8,128)(2,1)}), bf16[8,528,128]{2,1,0:T(8,128)(2,1)}, u32[]{:S(2)}, u32[]{:S(2)}) async-start(bf16[8,528,128]{2,1,0:T(8,128)(2,1)} %project.2), calls=%async_computation | async-start | bytes 2162688 | tf_op jit(solution)/shard_map/all_to_all | solution.py:432
  13.4 7.1 %project.3 = bf16[8,528,128]{2,1,0:T(8,128)(2,1)} custom-call(s32[8]{0:T(128)} %lengths_ref.6, s32[8,1,32]{2,1,0:T(1,128)} %chosen_ref.3, bf16[8,128,2048]{2,1,0:T(8,128)(2,1)} %tokens_ref.3, bf16[2048,512]{1,0:T(8,128)(2,1)} %wq_ref.3, bf16[2048,256]{1,0:T(8,128)(2,1)} %wk_ref.3, bf16[2048,256]{1,0:T(8,128)(2,1)} %wv_ref.3), custom_call_target="tpu_custom_call" | custom-call | flops 2147483648 | bytes 7372800 | tf_op jit(solution)/shard_map/project/pallas_call | solution.py:189
  20.5 0.0 copy-start
  20.5 8.0 %all-to-all-done.refs_0_ = bf16[8,528,128]{2,1,0:T(8,128)(2,1)} async-done(((bf16[8,528,128]{2,1,0:T(8,128)(2,1)}), bf16[8,528,128]{2,1,0:T(8,128)(2,1)}, u32[]{:S(2)}, u32[]{:S(2)}) %all-to-all-start) | async-done | bytes 1081376 | tf_op jit(solution)/shard_map/all_to_all | solution.py:432
  28.5 3.6 %all-to-all-start.1 = ((bf16[8,528,128]{2,1,0:T(8,128)(2,1)}), bf16[8,528,128]{2,1,0:T(8,128)(2,1)S(1)}, u32[]{:S(2)}, u32[]{:S(2)}) async-start(bf16[8,528,128]{2,1,0:T(8,128)(2,1)} %project.3), calls=%async_computation.1 | async-start | bytes 2162688 | tf_op jit(solution)/shard_map/all_to_all | solution.py:432
  32.1 1.1 %fusion.1 = (bf16[8,128,128]{2,1,0:T(8,128)(2,1)S(1)}, bf16[8,128,128]{2,1,0:T(8,128)(2,1)S(1)}) fusion(bf16[8,528,128]{2,1,0:T(8,128)(2,1)} %all-to-all-done.refs_0_), kind=kLoop, calls=%fused_computation.4 | loop fusion | bytes 1048576 | tf_op jit(solution)/shard_map/slice | solution.py:451
  33.2 4.5 %collective-permute-start.1 = (bf16[8,128,128]{2,1,0:T(8,128)(2,1)S(1)}, bf16[8,128,128]{2,1,0:T(8,128)(2,1)S(1)}, u32[]{:S(2)}, u32[]{:S(2)}) collective-permute-start(bf16[8,128,128]{2,1,0:T(8,128)(2,1)S(1)} %get-tuple-element.13), channel_id=1, source_target_pairs={{0,16},{2,18},{4,20},{6,22},{8,24},{10,26},{12,28},{14,30},{1,17},... | collective-permute-start | bytes 786440 | tf_op jit(solution)/shard_map/ppermute | solution.py:441
  37.7 0.0 copy-done
  37.7 0.6 fusion
  38.9 0.1 pad_add_fusion.where_ref
  39.0 0.7 slice.22
  39.7 7.3 %all-to-all-done.1.refs_1_ = bf16[8,528,128]{2,1,0:T(8,128)(2,1)S(1)} async-done(((bf16[8,528,128]{2,1,0:T(8,128)(2,1)}), bf16[8,528,128]{2,1,0:T(8,128)(2,1)S(1)}, u32[]{:S(2)}, u32[]{:S(2)}) %all-to-all-start.1) | async-done | bytes 1081376 | tf_op jit(solution)/shard_map/all_to_all | solution.py:432
  47.1 2.2 %collective-permute-done.1.far_ref = bf16[8,128,128]{2,1,0:T(8,128)(2,1)S(1)} collective-permute-done((bf16[8,128,128]{2,1,0:T(8,128)(2,1)S(1)}, bf16[8,128,128]{2,1,0:T(8,128)(2,1)S(1)}, u32[]{:S(2)}, u32[]{:S(2)}) %collective-permute-start.1) | collective-permute-done | bytes 262176 | tf_op jit(solution)/shard_map/ppermute | solution.py:441
  49.3 10.9 %attend.1 = bf16[8,512,128]{2,1,0:T(8,128)(2,1)S(1)} custom-call(s32[8]{0:T(128)S(1)} %copy-done, s32[2]{0:T(128)S(1)} %pad_add_fusion.where_ref, s32[4096]{0:T(1024)S(1)} %convert.2.list_ref, bf16[8,128,128]{2,1,0:T(8,128)(2,1)S(1)} %collective-permute-done.1.far_ref, bf16[8,528,128]{2,1,0:T(8,128)(2,1)} %all-to-all-done.refs_0_, ...), custom_call_target="tpu_custom_call" | custom-call | flops 2147483648 | bytes 3145728 | tf_op jit(solution)/shard_map/attend/pallas_call | solution.py:322
  60.3 0.0 copy-start.1
  60.3 17.9 %all_to_all.15.own_ref = bf16[8,512,128]{2,1,0:T(8,128)(2,1)S(1)} all-to-all(bf16[8,512,128]{2,1,0:T(8,128)(2,1)S(1)} %attend.1), channel_id=1, replica_groups={{0,2,4,6,8,10,12,14},{16,18,20,22,24,26,28,30},{1,3,5,7,9,11,13,15},{17..., dimensions={0} | all-to-all | bytes 2097152 | tf_op jit(solution)/shard_map/all_to_all | solution.py:432
  78.2 0.0 collective-permute-start.2
  78.2 2.8 %collective-permute-done.2.other_ref = bf16[8,512,128]{2,1,0:T(8,128)(2,1)} collective-permute-done((bf16[8,512,128]{2,1,0:T(8,128)(2,1)S(1)}, bf16[8,512,128]{2,1,0:T(8,128)(2,1)}, u32[]{:S(2)}, u32[]{:S(2)}) %collective-permute-start.2) | collective-permute-done | bytes 1048608 | tf_op jit(solution)/shard_map/ppermute | solution.py:463
  81.0 0.0 copy-done.1
  81.0 4.6 %output_projection.1 = bf16[8,128,1024]{2,1,0:T(8,128)(2,1)} custom-call(s32[8]{0:T(128)S(1)} %copy-done, s32[1]{0:T(128)} %bitcast.side_ref, bf16[8,512,128]{2,1,0:T(8,128)(2,1)S(1)} %all_to_all.15.own_ref, bf16[8,512,128]{2,1,0:T(8,128)(2,1)} %collective-permute-done.2.other_ref, bf16[1024,1024]{1,0:T(8,128)(2,1)S(1)} %copy-done.1), custom_call_target="tpu_custom_call" | custom-call | flops 2147483648 | bytes 6291456 | tf_op jit(solution)/shard_map/output_projection/pallas_call | solution.py:390
  (4 shorter events, 0.0 us)
Async XLA Ops:
  7.2 21.4 %all-to-all-start = ((bf16[8,528,128]{2,1,0:T(8,128)(2,1)}), bf16[8,528,128]{2,1,0:T(8,128)(2,1)}, u32[]{:S(2)}, u32[]{:S(2)}) async-start(bf16[8,528,128]{2,1,0:T(8,128)(2,1)} %project.2), calls=%async_computation | async-start | bytes 2162688 | tf_op jit(solution)/shard_map/all_to_all | solution.py:432
  20.5 17.2 %copy-start = (s32[8]{0:T(128)S(1)}, s32[8]{0:T(128)}, u32[]{:S(2)}) copy-start(s32[8]{0:T(128)} %lengths_ref.6) | copy-start | bytes 100
  28.5 18.5 %all-to-all-start.1 = ((bf16[8,528,128]{2,1,0:T(8,128)(2,1)}), bf16[8,528,128]{2,1,0:T(8,128)(2,1)S(1)}, u32[]{:S(2)}, u32[]{:S(2)}) async-start(bf16[8,528,128]{2,1,0:T(8,128)(2,1)} %project.3), calls=%async_computation.1 | async-start | bytes 2162688 | tf_op jit(solution)/shard_map/all_to_all | solution.py:432
  33.2 16.2 %collective-permute-start.1 = (bf16[8,128,128]{2,1,0:T(8,128)(2,1)S(1)}, bf16[8,128,128]{2,1,0:T(8,128)(2,1)S(1)}, u32[]{:S(2)}, u32[]{:S(2)}) collective-permute-start(bf16[8,128,128]{2,1,0:T(8,128)(2,1)S(1)} %get-tuple-element.13), channel_id=1, source_target_pairs={{0,16},{2,18},{4,20},{6,22},{8,24},{10,26},{12,28},{14,30},{1,17},... | collective-permute-start | bytes 786440 | tf_op jit(solution)/shard_map/ppermute | solution.py:441
  60.3 20.7 %copy-start.1 = (bf16[1024,1024]{1,0:T(8,128)(2,1)S(1)}, bf16[1024,1024]{1,0:T(8,128)(2,1)}, u32[]{:S(2)}) copy-start(bf16[1024,1024]{1,0:T(8,128)(2,1)} %w_ref.1) | copy-start | bytes 6291460
  78.2 2.8 %collective-permute-start.2 = (bf16[8,512,128]{2,1,0:T(8,128)(2,1)S(1)}, bf16[8,512,128]{2,1,0:T(8,128)(2,1)}, u32[]{:S(2)}, u32[]{:S(2)}) collective-permute-start(bf16[8,512,128]{2,1,0:T(8,128)(2,1)S(1)} %all_to_all.15.own_ref), channel_id=1, source_target_pairs={{0,1},{1,0},{2,3},{3,2},{4,5},{5,4},{6,7},{7,6},{8,9},{9,8},{10,11... | collective-permute-start | bytes 3145736 | tf_op jit(solution)/shard_map/ppermute | solution.py:463

commit v3 on v2

--- a/solution.py
+++ b/solution.py
@@ -7,13 +7,13 @@
 from jax.experimental.pallas import tpu as pltpu
 from jax.sharding import PartitionSpec as P
 
+
 HEADS = 16
 KV_HEADS = 8
 HEAD_DIM = 64
 CAP = 4
 META_ROWS = 16
 LANES = 128
-GROUP = 4
 VMEM_MOST = 63 << 20
 HBM = pltpu.HBM
 
@@ -118,8 +118,8 @@
 
 
 def project_kernel(
-    lengths_ref, chosen_ref, tokens_ref, wq_ref, wk_ref, wv_ref, out_ref,
-    order_ref, meta_ref, rows_ref, wq_buf, wk_buf, wv_buf, row_sems, w_sems,
+    lengths_in, chosen_in, tokens_ref, wq_ref, wk_ref, wv_ref, out_ref,
+    lengths_ref, chosen_ref, order_ref, meta_ref, rows_ref, wq_buf, wk_buf, wv_buf, row_sems, w_sems,
     *, ranks, slots, kv_local, select,
 ):
     seq_count = chosen_ref.shape[0]
@@ -129,6 +129,13 @@
         pltpu.make_async_copy(wk_ref, wk_buf, w_sems.at[1]),
         pltpu.make_async_copy(wv_ref, wv_buf, w_sems.at[2]),
     ]
+    small = [
+        pltpu.make_async_copy(lengths_in, lengths_ref, w_sems.at[3]),
+        pltpu.make_async_copy(chosen_in, chosen_ref, w_sems.at[4]),
+    ]
+    for load in small + loads[1:]:
+        load.start()
+    small[0].wait()
     order_by_length(lengths_ref, order_ref, seq_count)
     fetch = [
         pltpu.make_async_copy(
@@ -136,12 +143,9 @@
         )
         for i, rank in enumerate(ranks)
     ]
-    for f in fetch[:2]:
+    for f in fetch[:2] + loads[:1] + fetch[2:]:
         f.start()
-    for load in loads:
-        load.start()
-    for f in fetch[2:]:
-        f.start()
+    small[1].wait()
     meta_ref[...] = jnp.zeros(meta_ref.shape, jnp.float32)
     for s in range(seq_count):
         meta_ref[s:s + 1, :select] = chosen_ref[s].astype(jnp.float32)
@@ -159,15 +163,18 @@
         tile = tile.astype(jnp.bfloat16)
         for h in range(kv_local):
             out_ref[p * kv_local + h, slots * 2 * blk:, :] = tile
-    for load in loads:
-        load.wait()
     for first in range(0, len(ranks), 2):
         fetch[first].wait()
         fetch[first + 1].wait()
         rows = rows_ref[first * blk:(first + 2) * blk, :]
-        q = jnp.dot(rows, wq_buf[...], preferred_element_type=jnp.float32).astype(jnp.bfloat16)
+        if first == 0:
+            loads[1].wait()
+            loads[2].wait()
         k = jnp.dot(rows, wk_buf[...], preferred_element_type=jnp.float32).astype(jnp.bfloat16)
         v = jnp.dot(rows, wv_buf[...], preferred_element_type=jnp.float32).astype(jnp.bfloat16)
+        if first == 0:
+            loads[0].wait()
+        q = jnp.dot(rows, wq_buf[...], preferred_element_type=jnp.float32).astype(jnp.bfloat16)
         for h in range(kv_local):
             q_h = q[:, h * LANES:(h + 1) * LANES]
             kv_h = jnp.concatenate(
@@ -190,14 +197,12 @@
         functools.partial(
             project_kernel, ranks=ranks, slots=slots, kv_local=kv_local, select=chosen.shape[2]
         ),
-        in_specs=[
-            pl.BlockSpec(memory_space=pltpu.SMEM),
-            pl.BlockSpec(memory_space=pltpu.VMEM),
-            hbm, hbm, hbm, hbm,
-        ],
+        in_specs=[hbm] * 6,
         out_specs=pl.BlockSpec(memory_space=pltpu.VMEM),
         out_shape=jax.ShapeDtypeStruct((dests, rows, LANES), jnp.bfloat16),
         scratch_shapes=[
+            pltpu.SMEM((seq_count,), jnp.int32),
+            pltpu.VMEM(chosen.shape, jnp.int32),
             pltpu.SMEM((seq_count,), jnp.int32),
             pltpu.VMEM((seq_count, LANES), jnp.float32),
             pltpu.VMEM((len(ranks) * blk, width), jnp.bfloat16),
@@ -205,7 +210,7 @@
             pltpu.VMEM(w_key.shape, jnp.bfloat16),
             pltpu.VMEM(w_value.shape, jnp.bfloat16),
             pltpu.SemaphoreType.DMA((len(ranks),)),
-            pltpu.SemaphoreType.DMA((3,)),
+            pltpu.SemaphoreType.DMA((5,)),
         ],
         compiler_params=pltpu.CompilerParams(vmem_limit_bytes=VMEM_MOST),
         cost_estimate=pl.CostEstimate(
@@ -218,30 +223,46 @@
 
 
 def attend_kernel(
-    lengths_ref, where_ref, list_ref, far_ref, *refs, slots, split, planes, blocks, blk, stride,
+    lengths_ref, where_ref, list_ref, *refs, early, split, planes, blocks, blk, stride, sizes,
 ):
-    parts = slots // split
-    arrived, near, (out_ref, order_ref, q_buf, kv_buf, sems) = refs[:parts], refs[parts:-5], refs[-5:]
     plane, start = where_ref[0], where_ref[1]
-    copies = []
-    for j in range(slots):
-        part, base = arrived[j // split], j % split * 2 * blk
-        copies.append((part.at[:, pl.ds(base, blk), :], q_buf.at[j]))
-        copies.append((part.at[:, pl.ds(base + blk, blk), :], kv_buf.at[j, pl.ds(start, blocks)]))
-    for j, ref in enumerate((far_ref,) + near):
-        copies.append((ref, kv_buf.at[j, pl.ds(blocks - start, blocks)]))
-    copies = [pltpu.make_async_copy(a, b, sems.at[i]) for i, (a, b) in enumerate(copies)]
-    for copy in copies:
-        copy.start()
-    order_by_length(lengths_ref, order_ref, lengths_ref.shape[0])
+    first_half = start == 0
+    if early:
+        arrived, out_ref, order_ref, q_buf, kv_buf, o_buf, sems, out_sem = refs
+        part = 0
+    else:
+        own, arrived = refs[0], refs[1]
+        far = refs[2:2 + split]
+        out_ref, order_ref, q_buf, kv_buf, o_buf, sems, out_sem = refs[3 + split:]
+        part = jnp.where(first_half, 1, 0)
+
+    def loads(source, remote):
+        pairs = []
+        for j in range(split):
+            base = j * 2 * blk
+            pairs.append((source.at[:, pl.ds(base, blk), :], q_buf.at[j]))
+            at = kv_buf.at[j, pl.ds(blocks if remote else 0, blocks)]
+            pairs.append((source.at[:, pl.ds(base + blk, blk), :], at))
+            if remote:
+                pairs.append((far[j], kv_buf.at[j, pl.ds(0, blocks)]))
+        return [pltpu.make_async_copy(a, b, sems.at[i]) for i, (a, b) in enumerate(pairs)]
+
+    def fetch(source, remote):
+        copies = loads(source, remote)
+        for copy in copies:
+            copy.start()
+        for copy in copies:
+            copy.wait()
+
     lane = lax.broadcasted_iota(jnp.int32, (blk, LANES), 1)
     low = lane < HEAD_DIM
+    row = lax.broadcasted_iota(jnp.int32, (2 * blk, blk), 0) % blk
+    col = lax.broadcasted_iota(jnp.int32, (2 * blk, blk), 1)
     scale = HEAD_DIM ** -0.5
-    for copy in copies:
-        copy.wait()
 
     def list_at(j, b):
-        return ((j // split * blocks + b) * split + j % split) * LANES
+        kind = 0 if early else part * blocks
+        return ((kind + b) * split + j) * LANES
 
     def head_rows(j, b):
         q = q_buf[j, b].astype(jnp.float32)
@@ -249,98 +270,112 @@
         q0 = jnp.where(low, q, 0.0)
         return (jnp.concatenate([q0, q1], axis=0) * scale).astype(jnp.bfloat16)
 
-    def body(j, b, length, groups):
+    def body(j, b, length, total):
         meta = list_at(j, b)
         count = list_ref[meta + stride]
         q2 = head_rows(j, b)
-        total = groups * GROUP
-        kvs = []
-        for t in range(total):
-            c = jnp.maximum(list_ref[meta + t], 0)
-            kvs.append(kv_buf[j, c])
-        kv = jnp.concatenate(kvs, axis=0)
+        kv = jnp.concatenate(
+            [kv_buf[j, jnp.maximum(list_ref[meta + t], 0)] for t in range(total)], axis=0
+        )
         s = lax.dot_general(q2, kv, (((1,), (1,)), ((), ())), preferred_element_type=jnp.float32)
-        row = lax.broadcasted_iota(jnp.int32, (2 * blk, blk), 0) % blk
-        col = lax.broadcasted_iota(jnp.int32, (2 * blk, blk), 1)
         parts = []
         for t in range(total):
-            part = s[:, t * blk:(t + 1) * blk]
+            piece = s[:, t * blk:(t + 1) * blk]
             if t == 0:
-                part = jnp.where(col <= row, part, -1e30)
+                piece = jnp.where(col <= row, piece, -1e30)
             else:
-                part = jnp.where(t < count, part, -1e30)
-            parts.append(part)
+                piece = jnp.where(t < count, piece, -1e30)
+            parts.append(piece)
         peak = parts[0]
-        for part in parts[1:]:
-            peak = jnp.maximum(peak, part)
+        for piece in parts[1:]:
+            peak = jnp.maximum(peak, piece)
         m = jnp.max(peak, axis=1, keepdims=True)
-        exps = [jnp.exp(part - m) for part in parts]
-        acc = exps[0]
-        for e in exps[1:]:
-            acc = acc + e
-        denom = jnp.sum(acc, axis=1, keepdims=True)
-        p = jnp.concatenate([e.astype(jnp.bfloat16) for e in exps], axis=1)
-        o = jnp.dot(p, kv, preferred_element_type=jnp.float32) / denom
-        o = jnp.where(low, pltpu.roll(o[:blk], HEAD_DIM, 1), o[blk:])
+        p = jnp.concatenate([jnp.exp(piece - m).astype(jnp.bfloat16) for piece in parts], axis=1)
+        low_rows = lax.broadcasted_iota(jnp.int32, kv.shape, 1) < HEAD_DIM
+        values = jnp.where(low_rows, jnp.ones_like(kv), kv)
+        o = jnp.dot(p, values, preferred_element_type=jnp.float32)
+        turned = pltpu.roll(o, HEAD_DIM, 1)
+        o = jnp.where(low, turned[:blk] / o[:blk], o[blk:] / turned[blk:])
         pos = (start + b) * blk + lax.broadcasted_iota(jnp.int32, (blk, LANES), 0)
-        out_ref[b, pl.ds(pl.multiple_of(j * blk, blk), blk), :] = jnp.where(
+        o_buf[b, pl.ds(pl.multiple_of(j * blk, blk), blk), :] = jnp.where(
             pos < length, o, 0.0
         ).astype(jnp.bfloat16)
 
-    @pl.loop(0, slots * blocks // 2)
-    def _(step):
-        j, b = step // (blocks // 2), step % (blocks // 2) * 2
-        rank = j * planes + jnp.where(j % 2 == 0, plane, planes - 1 - plane)
-        length = lengths_ref[order_ref[rank]]
-        live = (start + b) * blk < length
-
-        @pl.when(live)
-        def _():
+    def run():
+        order_by_length(lengths_ref, order_ref, lengths_ref.shape[0])
+
+        @pl.loop(0, split * blocks // 2)
+        def _(step):
+            j, b = step // (blocks // 2), step % (blocks // 2) * 2
+            slot = part * split + j
+            rank = slot * planes + jnp.where(slot % 2 == 0, plane, planes - 1 - plane)
+            length = lengths_ref[order_ref[rank]]
             need = jnp.maximum(
                 list_ref[list_at(j, b) + stride], list_ref[list_at(j, b + 1) + stride]
             )
-            for groups in range(1, -(-2 * blocks // GROUP) + 1):
-                @pl.when((need > (groups - 1) * GROUP) & (need <= groups * GROUP))
+            live = (start + b) * blk < length
+            less = 0
+            for size in sizes:
+                @pl.when(live & (need > less) & (need <= size))
                 def _():
-                    body(j, b, length, groups)
-                    body(j, b + 1, length, groups)
-
-        @pl.when(jnp.logical_not(live))
+                    body(j, b, length, size)
+                    body(j, b + 1, length, size)
+
+                less = size
+
+        at = pl.ds(0 if early else pl.multiple_of(part * split * blk, split * blk), split * blk)
+        store = pltpu.make_async_copy(o_buf, out_ref.at[:, at, :], out_sem)
+        store.start()
+        store.wait()
+
+    if early:
+        @pl.when(first_half)
         def _():
-            zero = jnp.zeros((blk, LANES), jnp.bfloat16)
-            out_ref[b, pl.ds(pl.multiple_of(j * blk, blk), blk), :] = zero
-            out_ref[b + 1, pl.ds(pl.multiple_of(j * blk, blk), blk), :] = zero
-
-
-def attend(arrived, from_half, lengths, where, lists, split, planes, blk, stride):
-    blocks = arrived[0].shape[0]
-    slots = split * len(arrived)
+            fetch(arrived, False)
+            run()
+    else:
+        @pl.when(first_half)
+        def _():
+            fetch(arrived, False)
+
+        @pl.when(jnp.logical_not(first_half))
+        def _():
+            fetch(own, True)
+
+        run()
+
+
+def attend(lengths, where, lists, operands, early, split, planes, blk, stride):
+    blocks = operands[0].shape[0]
     smem = pl.BlockSpec(memory_space=pltpu.SMEM)
-    vmem = pl.BlockSpec(memory_space=pltpu.VMEM)
     anywhere = pl.BlockSpec(memory_space=pl.ANY)
-    far, *near = from_half
+    most = blocks if early else 2 * blocks
+    sizes = tuple(n for n in (2, 4, 6, 8, 10, 12, 16) if n < most) + (most,)
     return pl.pallas_call(
         functools.partial(
-            attend_kernel, slots=slots, split=split, planes=planes, blocks=blocks, blk=blk,
-            stride=stride,
+            attend_kernel, early=early, split=split, planes=planes, blocks=blocks, blk=blk,
+            stride=stride, sizes=sizes,
         ),
-        in_specs=[smem, smem, smem] + [anywhere] * (len(from_half) + len(arrived)),
-        out_specs=vmem,
-        out_shape=jax.ShapeDtypeStruct((blocks, slots * blk, LANES), jnp.bfloat16),
+        in_specs=[smem, smem, smem] + [anywhere] * len(operands),
+        out_specs=anywhere,
+        out_shape=jax.ShapeDtypeStruct((blocks, 2 * split * blk, LANES), jnp.bfloat16),
         scratch_shapes=[
             pltpu.SMEM(lengths.shape, jnp.int32),
-            pltpu.VMEM((slots, blocks, blk, LANES), jnp.bfloat16),
-            pltpu.VMEM((slots, 2 * blocks, blk, LANES), jnp.bfloat16),
-            pltpu.SemaphoreType.DMA((2 * slots + len(from_half),)),
+            pltpu.VMEM((split, blocks, blk, LANES), jnp.bfloat16),
+            pltpu.VMEM((split, most, blk, LANES), jnp.bfloat16),
+            pltpu.VMEM((blocks, split * blk, LANES), jnp.bfloat16),
+            pltpu.SemaphoreType.DMA((3 * split,)),
+            pltpu.SemaphoreType.DMA,
         ],
+        input_output_aliases={} if early else {2 + len(operands): 0},
         compiler_params=pltpu.CompilerParams(vmem_limit_bytes=40 << 20),
         cost_estimate=pl.CostEstimate(
-            flops=4 * 2 * blk * blk * LANES * blocks * blocks // 2 * slots,
+            flops=4 * 2 * blk * blk * LANES * blocks * blocks * split,
             transcendentals=0,
             bytes_accessed=3 << 20,
         ),
-        name="attend",
-    )(lengths, where, lists, far, *arrived, *near)
+        name="attend_early" if early else "attend",
+    )(lengths, where, lists, *operands)
 
 
 def output_kernel(
@@ -370,8 +405,11 @@
         o = o + jnp.dot(
             theirs, w_buf[pl.ds(other_at, half), :], preferred_element_type=jnp.float32
         )
-        rows_buf[rank:rank + 2] = o.astype(jnp.bfloat16).reshape(2, blk, -1)
         for r in (rank, rank + 1):
+            live = side_ref[1] < lengths_ref[order_ref[r]]
+            rows_buf[r] = jnp.where(
+                live, o[(r - rank) * blk:(r - rank + 1) * blk], 0.0
+            ).astype(jnp.bfloat16)
             store = pltpu.make_async_copy(
                 rows_buf.at[r], out_ref.at[order_ref[r]], out_sems.at[r]
             )
@@ -446,22 +484,34 @@
     arrived_a = exchange(sent_a)
     later, _ = lax.optimization_barrier((lengths, sent_a))
     sent_b = project(tokens, w_query, w_key, w_value, chosen, later, groups[1], split, kv_local)
-    from_half = []
-    for j in range(split):
-        kv = arrived_a[:, (2 * j + 1) * blk:(2 * j + 2) * blk, :]
-        if j == 0:
-            from_half.append(to_second_half(kv))
-        else:
-            longer = jnp.sum((lengths > half * blk).astype(jnp.int32)) > j * planes
-            from_half.append(lax.cond(longer, to_second_half, lambda x: x, kv))
+    lists_a = lists_of(arrived_a)
+    started = attend(
+        lengths, where, lists_a.reshape(-1), [arrived_a], True, split, planes, blk, select
+    )
+
+    def keys_of(arrived, j):
+        return arrived[:, (2 * j + 1) * blk:(2 * j + 2) * blk, :]
+
+    from_half = [to_second_half(keys_of(arrived_a, 0))]
+    for j in range(1, split):
+        longer = jnp.sum((lengths > half * blk).astype(jnp.int32)) > j * planes
+        from_half.append(
+            lax.cond(
+                longer,
+                lambda x: to_second_half(keys_of(x, j)),
+                lambda x: jnp.zeros((half, blk, LANES), x.dtype),
+                arrived_a,
+            )
+        )
     arrived_b = exchange(sent_b)
-    lists = jnp.concatenate([lists_of(arrived_a), lists_of(arrived_b)]).reshape(-1)
+    lists = jnp.concatenate([lists_a, lists_of(arrived_b)]).reshape(-1)
     attended = attend(
-        [arrived_a, arrived_b], from_half, lengths, where, lists, split, planes, blk, select
+        lengths, where, lists, [arrived_a, arrived_b] + from_half + [started], False, split,
+        planes, blk, select,
     )
     own = exchange(attended)
     other = lax.ppermute(own, "tp", [(0, 1), (1, 0)])
-    side = lax.axis_index("tp").astype(jnp.int32)[None]
+    side = jnp.stack([lax.axis_index("tp").astype(jnp.int32), here * blk])
     return output_projection(own, other, w_output, lengths, side, planes, kv_local, blk)
 
 
@@ -499,21 +549,27 @@
 
 def solution(mesh):
     def run(tokens, w_query, w_key, w_value, w_output, chosen, lengths):
-        body = per_device if fits(mesh, tokens, w_key, chosen) else per_device_general
-        return jax.shard_map(
-            body,
-            mesh=mesh,
-            in_specs=(
-                P(None, "kv", None),
-                P(None, "tp"),
-                P(None, "tp"),
-                P(None, "tp"),
-                P(None, "tp"),
-                P(None, "kv", None),
-                P(),
-            ),
-            out_specs=P(None, "kv", "tp"),
-            check_vma=False,
-        )(tokens, w_query, w_key, w_value, w_output, chosen, lengths)
+        def sharded(body):
+            return jax.shard_map(
+                body,
+                mesh=mesh,
+                in_specs=(
+                    P(None, "kv", None),
+                    P(None, "tp"),
+                    P(None, "tp"),
+                    P(None, "tp"),
+                    P(None, "tp"),
+                    P(None, "kv", None),
+                    P(),
+                ),
+                out_specs=P(None, "kv", "tp"),
+                check_vma=False,
+            )
+
+        arrays = (tokens, w_query, w_key, w_value, w_output, chosen, lengths)
+        if not fits(mesh, tokens, w_key, chosen):
+            return sharded(per_device_general)(*arrays)
+
+        return sharded(per_device)(*arrays)
 
     return run

time: 86.3 us -> 86.5 us (level)
  waiting for transfers between devices: 20.4 us -> 18.6 us
    ppermute x1, waiting for transfers between devices: 2.22 us -> 0.01 us  [to_second_half(): return lax.ppermute(x, 'kv', [(i, i + half) for i in range(half)])]
    pallas_call x1 -> x2, Pallas kernels: 10.9 us -> 12.5 us  [attend(): pl.pallas_call(functools.partial(attend_kernel, early=early, split=split,...]
    pallas_call x2, Pallas kernels: 14.2 us -> 13.1 us  [project(): pl.pallas_call(functools.partial(project_kernel, ranks=ranks, slots=slots...]
    slice x3 -> x1, local copies, waits for them, and re-layouts: 1.8 us -> 0.97 us  [keys_of(): return arrived[:, (2 * j + 1) * blk:(2 * j + 2) * blk, :]]
  transfers between devices with their start and end apart: 4 -> 4, of which waited for: 4 -> 3; matrix products, arithmetic and copies ran while one was open for 3% -> 4% of each run, Pallas kernels for 8% -> 17%
where the time goes in v3:
time: 86.5 us; the launch traced here: 86 us
  Pallas kernels  30.2 us (35%)
  blocking collectives  18.7 us (22%)
  waiting for transfers between devices  18.6 us (22%)
  starting transfers between devices  14.3 us (17%)
  local copies, waits for them, and re-layouts  1.73 us (2%)
  other arithmetic  1.54 us (2%)
  between operations  0.94 us (1%)
    all_to_all x1, blocking collectives, exchange(): lax.all_to_all(x, 'kv', split_axis=0, concat_axis=0, tiled=True, axis_ind...  18.7 us
    all_to_all x2, waiting for transfers between devices, exchange(): lax.all_to_all(x, 'kv', split_axis=0, concat_axis=0, tiled=True, axis_ind...  15.9 us
    pallas_call x2, Pallas kernels, project(): pl.pallas_call(functools.partial(project_kernel, ranks=ranks, slots=slots...  13.1 us
    pallas_call x2, Pallas kernels, attend(): pl.pallas_call(functools.partial(attend_kernel, early=early, split=split,...  12.5 us
    all_to_all x2, starting transfers between devices, exchange(): lax.all_to_all(x, 'kv', split_axis=0, concat_axis=0, tiled=True, axis_ind...  9.78 us
    pallas_call x1, Pallas kernels, output_projection(): pl.pallas_call(functools.partial(output_kernel, planes=planes, kv_local=k...  4.62 us
    ppermute x1, starting transfers between devices, to_second_half(): return lax.ppermute(x, 'kv', [(i, i + half) for i in range(half)])  4.51 us
    ppermute x1, waiting for transfers between devices, per_device(): other = lax.ppermute(own, 'tp', [(0, 1), (1, 0)])  2.71 us
  transfers between devices with their start and end apart: 4, of which 3 were waited for; matrix products, arithmetic and copies ran while one was open for 4% of the time, Pallas kernels for 17%

profile of v3, /device:TPU:0, one launch (start us, length us, event | category | flops | bytes accessed | tf_op | source)
XLA Modules:
  0.0 86.0 jit_solution(10810463456937245765)
XLA Ops:
  0.0 6.6 %project.2 = bf16[8,528,128]{2,1,0:T(8,128)(2,1)} custom-call(s32[8]{0:T(128)} %lengths_ref.5, s32[8,1,32]{2,1,0:T(1,128)} %chosen_in.3, bf16[8,128,2048]{2,1,0:T(8,128)(2,1)} %tokens_ref.3, bf16[2048,512]{1,0:T(8,128)(2,1)} %wq_ref.3, bf16[2048,256]{1,0:T(8,128)(2,1)} %wk_ref.3, bf16[2048,256]{1,0:T(8,128)(2,1)} %wv_ref.3), custom_call_target="tpu_custom_call" | custom-call | flops 2147483648 | bytes 7372800 | tf_op jit(solution)/shard_map/project/pallas_call | solution.py:196
  6.6 6.2 %all-to-all-start = ((bf16[8,528,128]{2,1,0:T(8,128)(2,1)}), bf16[8,528,128]{2,1,0:T(8,128)(2,1)}, u32[]{:S(2)}, u32[]{:S(2)}) async-start(bf16[8,528,128]{2,1,0:T(8,128)(2,1)} %project.2), calls=%async_computation | async-start | bytes 2162688 | tf_op jit(solution)/shard_map/all_to_all | solution.py:470
  12.8 6.5 %project.3 = bf16[8,528,128]{2,1,0:T(8,128)(2,1)} custom-call(s32[8]{0:T(128)} %lengths_ref.5, s32[8,1,32]{2,1,0:T(1,128)} %chosen_in.3, bf16[8,128,2048]{2,1,0:T(8,128)(2,1)} %tokens_ref.3, bf16[2048,512]{1,0:T(8,128)(2,1)} %wq_ref.3, bf16[2048,256]{1,0:T(8,128)(2,1)} %wk_ref.3, bf16[2048,256]{1,0:T(8,128)(2,1)} %wv_ref.3), custom_call_target="tpu_custom_call" | custom-call | flops 2147483648 | bytes 7372800 | tf_op jit(solution)/shard_map/project/pallas_call | solution.py:196
  19.3 0.0 copy-start
  19.3 8.6 %all-to-all-done.refs_0_ = bf16[8,528,128]{2,1,0:T(8,128)(2,1)} async-done(((bf16[8,528,128]{2,1,0:T(8,128)(2,1)}), bf16[8,528,128]{2,1,0:T(8,128)(2,1)}, u32[]{:S(2)}, u32[]{:S(2)}) %all-to-all-start) | async-done | bytes 1081376 | tf_op jit(solution)/shard_map/all_to_all | solution.py:470
  27.9 3.6 %all-to-all-start.1 = ((bf16[8,528,128]{2,1,0:T(8,128)(2,1)}), bf16[8,528,128]{2,1,0:T(8,128)(2,1)S(1)}, u32[]{:S(2)}, u32[]{:S(2)}) async-start(bf16[8,528,128]{2,1,0:T(8,128)(2,1)} %project.3), calls=%async_computation.1 | async-start | bytes 2162688 | tf_op jit(solution)/shard_map/all_to_all | solution.py:470
  31.5 0.0 copy-done
  31.6 0.7 fusion
  32.9 0.1 pad_add_fusion.2.where_ref
  32.9 1.0 %slice.17 = bf16[8,128,128]{2,1,0:T(8,128)(2,1)S(1)} slice(bf16[8,528,128]{2,1,0:T(8,128)(2,1)} %all-to-all-done.refs_0_), slice={[0:8], [128:256], [0:128]} | slice | bytes 524288 | tf_op jit(solution)/shard_map/slice | solution.py:493
  33.9 4.5 %collective-permute-start.1 = (bf16[8,128,128]{2,1,0:T(8,128)(2,1)S(1)}, bf16[8,128,128]{2,1,0:T(8,128)(2,1)S(1)}, u32[]{:S(2)}, u32[]{:S(2)}) collective-permute-start(bf16[8,128,128]{2,1,0:T(8,128)(2,1)S(1)} %slice.17), channel_id=1, source_target_pairs={{0,16},{2,18},{4,20},{6,22},{8,24},{10,26},{12,28},{14,30},{1,17},... | collective-permute-start | bytes 786440 | tf_op jit(solution)/shard_map/ppermute | solution.py:479
  38.4 0.7 slice_convert_fusion.1
  39.2 7.3 %all-to-all-done.1.refs_1_ = bf16[8,528,128]{2,1,0:T(8,128)(2,1)S(1)} async-done(((bf16[8,528,128]{2,1,0:T(8,128)(2,1)}), bf16[8,528,128]{2,1,0:T(8,128)(2,1)S(1)}, u32[]{:S(2)}, u32[]{:S(2)}) %all-to-all-start.1) | async-done | bytes 1081376 | tf_op jit(solution)/shard_map/all_to_all | solution.py:470
  46.5 0.7 conditional.1
  46.5 0.7 broadcast.7
  47.2 8.2 %attend_early.1.refs_4_ = bf16[8,512,128]{2,1,0:T(8,128)(2,1)S(1)} custom-call(s32[8]{0:T(128)S(1)} %copy-done, s32[2]{0:T(128)S(1)} %pad_add_fusion.2.where_ref, s32[2048]{0:T(1024)S(1)} %bitcast.6, bf16[8,528,128]{2,1,0:T(8,128)(2,1)} %all-to-all-done.refs_0_), custom_call_target="tpu_custom_call" | custom-call | flops 2147483648 | bytes 3145728 | tf_op jit(solution)/shard_map/attend_early/pallas_call | solution.py:354
  55.5 0.0 collective-permute-done.1.refs_2_
  55.5 4.2 %attend.1 = bf16[8,512,128]{2,1,0:T(8,128)(2,1)S(1)} custom-call(s32[8]{0:T(128)S(1)} %copy-done, s32[2]{0:T(128)S(1)} %pad_add_fusion.2.where_ref, s32[4096]{0:T(1024)S(1)} %bitcast.7, bf16[8,528,128]{2,1,0:T(8,128)(2,1)} %all-to-all-done.refs_0_, bf16[8,528,128]{2,1,0:T(8,128)(2,1)S(1)} %all-to-all-done.1.refs_1_, ...), custom_call_target="tpu_custom_call", output_to_operand_aliasing={{}: (7, {})} | custom-call | flops 2147483648 | bytes 3145728 | tf_op jit(solution)/shard_map/attend/pallas_call | solution.py:354
  59.7 0.0 copy-start.1
  59.7 18.7 %all_to_all.18.own_ref = bf16[8,512,128]{2,1,0:T(8,128)(2,1)S(1)} all-to-all(bf16[8,512,128]{2,1,0:T(8,128)(2,1)S(1)} %attend.1), channel_id=1, replica_groups={{0,2,4,6,8,10,12,14},{16,18,20,22,24,26,28,30},{1,3,5,7,9,11,13,15},{17..., dimensions={0} | all-to-all | bytes 2097152 | tf_op jit(solution)/shard_map/all_to_all | solution.py:470
  78.5 0.0 collective-permute-start.2
  78.5 0.1 pad_add_fusion.1.side_ref
  78.6 2.7 %collective-permute-done.2.other_ref = bf16[8,512,128]{2,1,0:T(8,128)(2,1)} collective-permute-done((bf16[8,512,128]{2,1,0:T(8,128)(2,1)S(1)}, bf16[8,512,128]{2,1,0:T(8,128)(2,1)}, u32[]{:S(2)}, u32[]{:S(2)}) %collective-permute-start.2) | collective-permute-done | bytes 1048608 | tf_op jit(solution)/shard_map/ppermute | solution.py:513
  81.3 4.6 %output_projection.1 = bf16[8,128,1024]{2,1,0:T(8,128)(2,1)} custom-call(s32[8]{0:T(128)S(1)} %copy-done, s32[2]{0:T(128)S(1)} %pad_add_fusion.1.side_ref, bf16[8,512,128]{2,1,0:T(8,128)(2,1)S(1)} %all_to_all.18.own_ref, bf16[8,512,128]{2,1,0:T(8,128)(2,1)} %collective-permute-done.2.other_ref, bf16[1024,1024]{1,0:T(8,128)(2,1)S(1)} %copy-done.1), custom_call_target="tpu_custom_call" | custom-call | flops 2147483648 | bytes 6291456 | tf_op jit(solution)/shard_map/output_projection/pallas_call | solution.py:428
  (3 shorter events, 0.0 us)
Async XLA Ops:
  6.6 21.4 %all-to-all-start = ((bf16[8,528,128]{2,1,0:T(8,128)(2,1)}), bf16[8,528,128]{2,1,0:T(8,128)(2,1)}, u32[]{:S(2)}, u32[]{:S(2)}) async-start(bf16[8,528,128]{2,1,0:T(8,128)(2,1)} %project.2), calls=%async_computation | async-start | bytes 2162688 | tf_op jit(solution)/shard_map/all_to_all | solution.py:470
  19.3 12.3 %copy-start = (s32[8]{0:T(128)S(1)}, s32[8]{0:T(128)}, u32[]{:S(2)}) copy-start(s32[8]{0:T(128)} %lengths_ref.5) | copy-start | bytes 100
  27.9 18.5 %all-to-all-start.1 = ((bf16[8,528,128]{2,1,0:T(8,128)(2,1)}), bf16[8,528,128]{2,1,0:T(8,128)(2,1)S(1)}, u32[]{:S(2)}, u32[]{:S(2)}) async-start(bf16[8,528,128]{2,1,0:T(8,128)(2,1)} %project.3), calls=%async_computation.1 | async-start | bytes 2162688 | tf_op jit(solution)/shard_map/all_to_all | solution.py:470
  33.9 21.6 %collective-permute-start.1 = (bf16[8,128,128]{2,1,0:T(8,128)(2,1)S(1)}, bf16[8,128,128]{2,1,0:T(8,128)(2,1)S(1)}, u32[]{:S(2)}, u32[]{:S(2)}) collective-permute-start(bf16[8,128,128]{2,1,0:T(8,128)(2,1)S(1)} %slice.17), channel_id=1, source_target_pairs={{0,16},{2,18},{4,20},{6,22},{8,24},{10,26},{12,28},{14,30},{1,17},... | collective-permute-start | bytes 786440 | tf_op jit(solution)/shard_map/ppermute | solution.py:479
  59.7 21.5 %copy-start.1 = (bf16[1024,1024]{1,0:T(8,128)(2,1)S(1)}, bf16[1024,1024]{1,0:T(8,128)(2,1)}, u32[]{:S(2)}) copy-start(bf16[1024,1024]{1,0:T(8,128)(2,1)} %w_ref.1) | copy-start | bytes 6291460
  78.5 2.8 %collective-permute-start.2 = (bf16[8,512,128]{2,1,0:T(8,128)(2,1)S(1)}, bf16[8,512,128]{2,1,0:T(8,128)(2,1)}, u32[]{:S(2)}, u32[]{:S(2)}) collective-permute-start(bf16[8,512,128]{2,1,0:T(8,128)(2,1)S(1)} %all_to_all.18.own_ref), channel_id=1, source_target_pairs={{0,1},{1,0},{2,3},{3,2},{4,5},{5,4},{6,7},{7,6},{8,9},{9,8},{10,11... | collective-permute-start | bytes 3145736 | tf_op jit(solution)/shard_map/ppermute | solution.py:513

commit v4 on v3

--- a/solution.py
+++ b/solution.py
@@ -14,7 +14,6 @@
 CAP = 4
 META_ROWS = 16
 LANES = 128
-VMEM_MOST = 63 << 20
 HBM = pltpu.HBM
 
 
@@ -118,8 +117,8 @@
 
 
 def project_kernel(
-    lengths_in, chosen_in, tokens_ref, wq_ref, wk_ref, wv_ref, out_ref,
-    lengths_ref, chosen_ref, order_ref, meta_ref, rows_ref, wq_buf, wk_buf, wv_buf, row_sems, w_sems,
+    lengths_in, chosen_in, tokens_ref, wq_ref, wk_ref, wv_ref, sent_ref,
+    out_ref, sent_sems, lengths_ref, chosen_ref, order_ref, meta_ref, rows_ref, wq_buf, wk_buf, wv_buf, row_sems, w_sems,
     *, ranks, slots, kv_local, select,
 ):
     seq_count = chosen_ref.shape[0]
@@ -163,6 +162,7 @@
         tile = tile.astype(jnp.bfloat16)
         for h in range(kv_local):
             out_ref[p * kv_local + h, slots * 2 * blk:, :] = tile
+    stores = []
     for first in range(0, len(ranks), 2):
         fetch[first].wait()
         fetch[first + 1].wait()
@@ -186,9 +186,18 @@
                 base = j * 2 * blk
                 out_ref[p * kv_local + h, base:base + blk, :] = q_h[i * blk:(i + 1) * blk]
                 out_ref[p * kv_local + h, base + blk:base + 2 * blk, :] = kv_h[i * blk:(i + 1) * blk]
-
-
-def project(tokens, w_query, w_key, w_value, chosen, lengths, ranks, slots, kv_local):
+        if (first + 2) % slots == 0:
+            p = first // slots
+            at = pl.ds(p * kv_local, kv_local)
+            stores.append(
+                pltpu.make_async_copy(out_ref.at[at], sent_ref.at[at], sent_sems.at[p])
+            )
+            stores[-1].start()
+    for store in stores:
+        store.wait()
+
+
+def project(tokens, w_query, w_key, w_value, chosen, lengths, ranks, slots, kv_local, vmem):
     seq_count, blk, width = tokens.shape
     dests = len(ranks) // slots * kv_local
     rows = slots * 2 * blk + META_ROWS
@@ -198,9 +207,11 @@
             project_kernel, ranks=ranks, slots=slots, kv_local=kv_local, select=chosen.shape[2]
         ),
         in_specs=[hbm] * 6,
-        out_specs=pl.BlockSpec(memory_space=pltpu.VMEM),
+        out_specs=pl.BlockSpec(memory_space=pl.ANY),
         out_shape=jax.ShapeDtypeStruct((dests, rows, LANES), jnp.bfloat16),
         scratch_shapes=[
+            pltpu.VMEM((dests, rows, LANES), jnp.bfloat16),
+            pltpu.SemaphoreType.DMA((len(ranks) // slots,)),
             pltpu.SMEM((seq_count,), jnp.int32),
             pltpu.VMEM(chosen.shape, jnp.int32),
             pltpu.SMEM((seq_count,), jnp.int32),
@@ -212,7 +223,7 @@
             pltpu.SemaphoreType.DMA((len(ranks),)),
             pltpu.SemaphoreType.DMA((5,)),
         ],
-        compiler_params=pltpu.CompilerParams(vmem_limit_bytes=VMEM_MOST),
+        compiler_params=pltpu.CompilerParams(vmem_limit_bytes=vmem << 10),
         cost_estimate=pl.CostEstimate(
             flops=2 * len(ranks) * blk * width * 2 * kv_local * LANES,
             transcendentals=0,
@@ -228,31 +239,29 @@
     plane, start = where_ref[0], where_ref[1]
     first_half = start == 0
     if early:
-        arrived, out_ref, order_ref, q_buf, kv_buf, o_buf, sems, out_sem = refs
+        arrived, out_ref, order_ref, o_buf, out_sem = refs
         part = 0
     else:
         own, arrived = refs[0], refs[1]
         far = refs[2:2 + split]
-        out_ref, order_ref, q_buf, kv_buf, o_buf, sems, out_sem = refs[3 + split:]
+        out_ref, order_ref, o_buf, out_sem = refs[3 + split:]
         part = jnp.where(first_half, 1, 0)
 
-    def loads(source, remote):
-        pairs = []
-        for j in range(split):
-            base = j * 2 * blk
-            pairs.append((source.at[:, pl.ds(base, blk), :], q_buf.at[j]))
-            at = kv_buf.at[j, pl.ds(blocks if remote else 0, blocks)]
-            pairs.append((source.at[:, pl.ds(base + blk, blk), :], at))
-            if remote:
-                pairs.append((far[j], kv_buf.at[j, pl.ds(0, blocks)]))
-        return [pltpu.make_async_copy(a, b, sems.at[i]) for i, (a, b) in enumerate(pairs)]
-
-    def fetch(source, remote):
-        copies = loads(source, remote)
-        for copy in copies:
-            copy.start()
-        for copy in copies:
-            copy.wait()
+    def near_block(j, b, at):
+        rows = pl.ds(pl.multiple_of(j * 2 * blk + at, blk), blk)
+        if early:
+            return arrived[b, rows, :]
+        return jnp.where(first_half, arrived[b, rows, :], own[b, rows, :])
+
+    def key_block(j, c):
+        if early:
+            return near_block(j, c, blk)
+        near = near_block(j, jnp.maximum(c - start, 0), blk)
+        at = jnp.minimum(c, blocks - 1)
+        other = far[0][at]
+        for k in range(1, split):
+            other = jnp.where(j == k, far[k][at], other)
+        return jnp.where(c >= start, near, other)
 
     lane = lax.broadcasted_iota(jnp.int32, (blk, LANES), 1)
     low = lane < HEAD_DIM
@@ -265,7 +274,7 @@
         return ((kind + b) * split + j) * LANES
 
     def head_rows(j, b):
-        q = q_buf[j, b].astype(jnp.float32)
+        q = near_block(j, b, 0).astype(jnp.float32)
         q1 = jnp.where(low, pltpu.roll(q, HEAD_DIM, 1), 0.0)
         q0 = jnp.where(low, q, 0.0)
         return (jnp.concatenate([q0, q1], axis=0) * scale).astype(jnp.bfloat16)
@@ -275,7 +284,7 @@
         count = list_ref[meta + stride]
         q2 = head_rows(j, b)
         kv = jnp.concatenate(
-            [kv_buf[j, jnp.maximum(list_ref[meta + t], 0)] for t in range(total)], axis=0
+            [key_block(j, jnp.maximum(list_ref[meta + t], 0)) for t in range(total)], axis=0
         )
         s = lax.dot_general(q2, kv, (((1,), (1,)), ((), ())), preferred_element_type=jnp.float32)
         parts = []
@@ -329,25 +338,15 @@
         store.wait()
 
     if early:
-        @pl.when(first_half)
-        def _():
-            fetch(arrived, False)
-            run()
+        pl.when(first_half)(run)
     else:
-        @pl.when(first_half)
-        def _():
-            fetch(arrived, False)
-
-        @pl.when(jnp.logical_not(first_half))
-        def _():
-            fetch(own, True)
-
         run()
 
 
 def attend(lengths, where, lists, operands, early, split, planes, blk, stride):
     blocks = operands[0].shape[0]
     smem = pl.BlockSpec(memory_space=pltpu.SMEM)
+    vmem = pl.BlockSpec(memory_space=pltpu.VMEM)
     anywhere = pl.BlockSpec(memory_space=pl.ANY)
     most = blocks if early else 2 * blocks
     sizes = tuple(n for n in (2, 4, 6, 8, 10, 12, 16) if n < most) + (most,)
@@ -356,15 +355,14 @@
             attend_kernel, early=early, split=split, planes=planes, blocks=blocks, blk=blk,
             stride=stride, sizes=sizes,
         ),
-        in_specs=[smem, smem, smem] + [anywhere] * len(operands),
+        in_specs=[smem, smem, smem]
+        + [vmem] * (len(operands) - (0 if early else 1))
+        + ([] if early else [anywhere]),
         out_specs=anywhere,
         out_shape=jax.ShapeDtypeStruct((blocks, 2 * split * blk, LANES), jnp.bfloat16),
         scratch_shapes=[
             pltpu.SMEM(lengths.shape, jnp.int32),
-            pltpu.VMEM((split, blocks, blk, LANES), jnp.bfloat16),
-            pltpu.VMEM((split, most, blk, LANES), jnp.bfloat16),
             pltpu.VMEM((blocks, split * blk, LANES), jnp.bfloat16),
-            pltpu.SemaphoreType.DMA((3 * split,)),
             pltpu.SemaphoreType.DMA,
         ],
         input_output_aliases={} if early else {2 + len(operands): 0},
@@ -380,11 +378,9 @@
 
 def output_kernel(
     lengths_ref, side_ref, own_ref, other_ref, w_ref, out_ref,
-    order_ref, w_buf, rows_buf, sem, out_sems, *, planes, kv_local,
+    order_ref, rows_buf, out_sems, *, planes, kv_local,
 ):
     seq_count, blk = out_ref.shape[0], out_ref.shape[1]
-    load = pltpu.make_async_copy(w_ref, w_buf, sem)
-    load.start()
     order_by_length(lengths_ref, order_ref, seq_count)
     half = kv_local * LANES
     own_at = pl.multiple_of(side_ref[0] * half, half)
@@ -396,14 +392,13 @@
             [ref[p * kv_local + h, j * blk:(j + 1) * blk, :] for h in range(kv_local)], axis=1
         )
 
-    load.wait()
     stores = []
     for rank in range(0, seq_count, 2):
         mine = jnp.concatenate([rows(own_ref, rank), rows(own_ref, rank + 1)], axis=0)
         theirs = jnp.concatenate([rows(other_ref, rank), rows(other_ref, rank + 1)], axis=0)
-        o = jnp.dot(mine, w_buf[pl.ds(own_at, half), :], preferred_element_type=jnp.float32)
+        o = jnp.dot(mine, w_ref[pl.ds(own_at, half), :], preferred_element_type=jnp.float32)
         o = o + jnp.dot(
-            theirs, w_buf[pl.ds(other_at, half), :], preferred_element_type=jnp.float32
+            theirs, w_ref[pl.ds(other_at, half), :], preferred_element_type=jnp.float32
         )
         for r in (rank, rank + 1):
             live = side_ref[1] < lengths_ref[order_ref[r]]
@@ -427,14 +422,12 @@
     hbm = pl.BlockSpec(memory_space=HBM)
     return pl.pallas_call(
         functools.partial(output_kernel, planes=planes, kv_local=kv_local),
-        in_specs=[smem, smem, vmem, vmem, hbm],
+        in_specs=[smem, smem, vmem, vmem, vmem],
         out_specs=hbm,
         out_shape=jax.ShapeDtypeStruct((seq_count, blk, width), jnp.bfloat16),
         scratch_shapes=[
             pltpu.SMEM((seq_count,), jnp.int32),
-            pltpu.VMEM(w_output.shape, jnp.bfloat16),
             pltpu.VMEM((seq_count, blk, width), jnp.bfloat16),
-            pltpu.SemaphoreType.DMA,
             pltpu.SemaphoreType.DMA((seq_count,)),
         ],
         compiler_params=pltpu.CompilerParams(vmem_limit_bytes=40 << 20),
@@ -480,10 +473,12 @@
 
     here = lax.axis_index("kv").astype(jnp.int32)
     where = jnp.stack([here % half // kv_local, here // half * half])
-    sent_a = project(tokens, w_query, w_key, w_value, chosen, lengths, groups[0], split, kv_local)
+    sent_a = project(tokens, w_query, w_key, w_value, chosen, lengths, groups[0], split, kv_local, 64000)
     arrived_a = exchange(sent_a)
     later, _ = lax.optimization_barrier((lengths, sent_a))
-    sent_b = project(tokens, w_query, w_key, w_value, chosen, later, groups[1], split, kv_local)
+    sent_b = project(tokens, w_query, w_key, w_value, chosen, later, groups[1], split, kv_local, 61440)
+    long_count = jnp.sum((lengths > half * blk).astype(jnp.int32))
+    sent_b, long_count = lax.optimization_barrier((sent_b, long_count))
     lists_a = lists_of(arrived_a)
     started = attend(
         lengths, where, lists_a.reshape(-1), [arrived_a], True, split, planes, blk, select
@@ -494,10 +489,9 @@
 
     from_half = [to_second_half(keys_of(arrived_a, 0))]
     for j in range(1, split):
-        longer = jnp.sum((lengths > half * blk).astype(jnp.int32)) > j * planes
         from_half.append(
             lax.cond(
-                longer,
+                long_count > j * planes,
                 lambda x: to_second_half(keys_of(x, j)),
                 lambda x: jnp.zeros((half, blk, LANES), x.dtype),
                 arrived_a,
@@ -524,7 +518,7 @@
     if kv_local == 0 or kv_devices % (4 * kv_local) or kv_devices > 16 or chosen.shape[2] >= LANES:
         return False
     planes = kv_devices // 2 // kv_local
-    if seq_len // kv_devices != LANES or seq_count % (2 * planes) or seq_count % 4:
+    if seq_len // kv_devices != LANES or seq_count % (4 * planes):
         return False
     split = seq_count // planes // 2
     fits_half = (seq_count - 1) * seq_len // 4 // (split * planes) <= seq_len // 2

time: 86.5 us -> 85 us (0.983)
  waiting for transfers between devices: 18.6 us -> 20.4 us
  Pallas kernels: 30.2 us -> 28.8 us
  local copies, waits for them, and re-layouts: 1.73 us -> 0.77 us
    all_to_all x2, waiting for transfers between devices: 15.9 us -> 17.7 us  [exchange(): lax.all_to_all(x, 'kv', split_axis=0, concat_axis=0, tiled=True, axis_ind...]
    slice x1, local copies, waits for them, and re-layouts: 0.97 us -> 0.02 us  [keys_of(): return arrived[:, (2 * j + 1) * blk:(2 * j + 2) * blk, :]]
  transfers between devices with their start and end apart: 4 -> 4, of which waited for: 3 -> 3; matrix products, arithmetic and copies ran while one was open for 4% -> 2% of each run, Pallas kernels for 17% -> 16%
where the time goes in v4:
time: 85 us; the launch traced here: 84.7 us
  Pallas kernels  28.8 us (34%)
  waiting for transfers between devices  20.4 us (24%)
  blocking collectives  18.6 us (22%)
  starting transfers between devices  14.3 us (17%)
  between operations  0.94 us (1%)
    all_to_all x1, blocking collectives, exchange(): lax.all_to_all(x, 'kv', split_axis=0, concat_axis=0, tiled=True, axis_ind...  18.6 us
    all_to_all x2, waiting for transfers between devices, exchange(): lax.all_to_all(x, 'kv', split_axis=0, concat_axis=0, tiled=True, axis_ind...  17.7 us
    pallas_call x2, Pallas kernels, project(): pl.pallas_call(functools.partial(project_kernel, ranks=ranks, slots=slots...  12.7 us
    pallas_call x2, Pallas kernels, attend(): pl.pallas_call(functools.partial(attend_kernel, early=early, split=split,...  11.7 us
    all_to_all x2, starting transfers between devices, exchange(): lax.all_to_all(x, 'kv', split_axis=0, concat_axis=0, tiled=True, axis_ind...  9.78 us
    ppermute x1, starting transfers between devices, to_second_half(): return lax.ppermute(x, 'kv', [(i, i + half) for i in range(half)])  4.51 us
    pallas_call x1, Pallas kernels, output_projection(): pl.pallas_call(functools.partial(output_kernel, planes=planes, kv_local=k...  4.44 us
    ppermute x1, waiting for transfers between devices, per_device(): other = lax.ppermute(own, 'tp', [(0, 1), (1, 0)])  2.71 us
  transfers between devices with their start and end apart: 4, of which 3 were waited for; matrix products, arithmetic and copies ran while one was open for 2% of the time, Pallas kernels for 16%

profile of v4, /device:TPU:0, one launch (start us, length us, event | category | flops | bytes accessed | tf_op | source)
XLA Modules:
  0.0 84.7 jit_solution(16968989569442412900)
XLA Ops:
  0.0 6.3 %project.2 = bf16[8,528,128]{2,1,0:T(8,128)(2,1)} custom-call(s32[8]{0:T(128)} %lengths_ref.5, s32[8,1,32]{2,1,0:T(1,128)} %chosen_in.3, bf16[8,128,2048]{2,1,0:T(8,128)(2,1)} %tokens_ref.3, bf16[2048,512]{1,0:T(8,128)(2,1)} %wq_ref.3, bf16[2048,256]{1,0:T(8,128)(2,1)} %wk_ref.3, bf16[2048,256]{1,0:T(8,128)(2,1)} %wv_ref.3), custom_call_target="tpu_custom_call" | custom-call | flops 2147483648 | bytes 7372800 | tf_op jit(solution)/shard_map/project/pallas_call | solution.py:205
  6.3 0.0 copy-start
  6.3 6.2 %all-to-all-start = ((bf16[8,528,128]{2,1,0:T(8,128)(2,1)}), bf16[8,528,128]{2,1,0:T(8,128)(2,1)S(1)}, u32[]{:S(2)}, u32[]{:S(2)}) async-start(bf16[8,528,128]{2,1,0:T(8,128)(2,1)} %project.2), calls=%async_computation | async-start | bytes 2162688 | tf_op jit(solution)/shard_map/all_to_all | solution.py:463
  12.6 0.0 copy-done
  12.6 0.7 fusion
  13.2 6.3 %project.3 = bf16[8,528,128]{2,1,0:T(8,128)(2,1)} custom-call(s32[8]{0:T(128)} %lengths_ref.5, s32[8,1,32]{2,1,0:T(1,128)} %chosen_in.3, bf16[8,128,2048]{2,1,0:T(8,128)(2,1)} %tokens_ref.3, bf16[2048,512]{1,0:T(8,128)(2,1)} %wq_ref.3, bf16[2048,256]{1,0:T(8,128)(2,1)} %wk_ref.3, bf16[2048,256]{1,0:T(8,128)(2,1)} %wv_ref.3), custom_call_target="tpu_custom_call" | custom-call | flops 2147483648 | bytes 7372800 | tf_op jit(solution)/shard_map/project/pallas_call | solution.py:205
  19.6 8.0 %all-to-all-done.refs_0_ = bf16[8,528,128]{2,1,0:T(8,128)(2,1)S(1)} async-done(((bf16[8,528,128]{2,1,0:T(8,128)(2,1)}), bf16[8,528,128]{2,1,0:T(8,128)(2,1)S(1)}, u32[]{:S(2)}, u32[]{:S(2)}) %all-to-all-start) | async-done | bytes 1081376 | tf_op jit(solution)/shard_map/all_to_all | solution.py:463
  27.6 3.6 %all-to-all-start.1 = ((bf16[8,528,128]{2,1,0:T(8,128)(2,1)}), bf16[8,528,128]{2,1,0:T(8,128)(2,1)S(1)}, u32[]{:S(2)}, u32[]{:S(2)}) async-start(bf16[8,528,128]{2,1,0:T(8,128)(2,1)} %project.3), calls=%async_computation.1 | async-start | bytes 2162688 | tf_op jit(solution)/shard_map/all_to_all | solution.py:463
  31.2 0.0 copy-start.1
  31.9 0.1 pad_add_fusion.2.where_ref
  32.0 4.5 %collective-permute-start.1 = (bf16[8,128,128]{2,1,0:T(8,128)(2,1)S(1)}, bf16[8,128,128]{2,1,0:T(8,128)(2,1)S(1)}, u32[]{:S(2)}, u32[]{:S(2)}) collective-permute-start(bf16[8,128,128]{2,1,0:T(8,128)(2,1)S(1)} %slice.17), channel_id=1, source_target_pairs={{0,16},{2,18},{4,20},{6,22},{8,24},{10,26},{12,28},{14,30},{1,17},... | collective-permute-start | bytes 786440 | tf_op jit(solution)/shard_map/ppermute | solution.py:472
  36.5 9.6 %all-to-all-done.1.refs_1_ = bf16[8,528,128]{2,1,0:T(8,128)(2,1)S(1)} async-done(((bf16[8,528,128]{2,1,0:T(8,128)(2,1)}), bf16[8,528,128]{2,1,0:T(8,128)(2,1)S(1)}, u32[]{:S(2)}, u32[]{:S(2)}) %all-to-all-start.1) | async-done | bytes 1081376 | tf_op jit(solution)/shard_map/all_to_all | solution.py:463
  46.1 0.7 conditional.1
  46.1 0.7 broadcast.7
  46.9 0.0 copy-done.1
  46.9 7.4 %attend_early.1.refs_4_ = bf16[8,512,128]{2,1,0:T(8,128)(2,1)S(1)} custom-call(s32[8]{0:T(128)S(1)} %copy-done.1, s32[2]{0:T(128)S(1)} %pad_add_fusion.2.where_ref, s32[2048]{0:T(1024)S(1)} %bitcast.6, bf16[8,528,128]{2,1,0:T(8,128)(2,1)S(1)} %all-to-all-done.refs_0_), custom_call_target="tpu_custom_call" | custom-call | flops 2147483648 | bytes 3145728 | tf_op jit(solution)/shard_map/attend_early/pallas_call | solution.py:353
  54.2 0.0 collective-permute-done.1.refs_2_
  54.3 4.3 %attend.1 = bf16[8,512,128]{2,1,0:T(8,128)(2,1)S(1)} custom-call(s32[8]{0:T(128)S(1)} %copy-done.1, s32[2]{0:T(128)S(1)} %pad_add_fusion.2.where_ref, s32[4096]{0:T(1024)S(1)} %bitcast.7, bf16[8,528,128]{2,1,0:T(8,128)(2,1)S(1)} %all-to-all-done.refs_0_, bf16[8,528,128]{2,1,0:T(8,128)(2,1)S(1)} %all-to-all-done.1.refs_1_, ...), custom_call_target="tpu_custom_call", output_to_operand_aliasing={{}: (7, {})} | custom-call | flops 2147483648 | bytes 3145728 | tf_op jit(solution)/shard_map/attend/pallas_call | solution.py:353
  58.6 0.0 copy-start.2
  58.6 18.6 %all_to_all.18.own_ref = bf16[8,512,128]{2,1,0:T(8,128)(2,1)S(1)} all-to-all(bf16[8,512,128]{2,1,0:T(8,128)(2,1)S(1)} %attend.1), channel_id=1, replica_groups={{0,2,4,6,8,10,12,14},{16,18,20,22,24,26,28,30},{1,3,5,7,9,11,13,15},{17..., dimensions={0} | all-to-all | bytes 2097152 | tf_op jit(solution)/shard_map/all_to_all | solution.py:463
  77.3 0.0 collective-permute-start.2
  77.3 0.1 pad_add_fusion.1.side_ref
  77.3 2.7 %collective-permute-done.2.other_ref = bf16[8,512,128]{2,1,0:T(8,128)(2,1)} collective-permute-done((bf16[8,512,128]{2,1,0:T(8,128)(2,1)S(1)}, bf16[8,512,128]{2,1,0:T(8,128)(2,1)}, u32[]{:S(2)}, u32[]{:S(2)}) %collective-permute-start.2) | collective-permute-done | bytes 1048608 | tf_op jit(solution)/shard_map/ppermute | solution.py:507
  80.1 4.4 %output_projection.1 = bf16[8,128,1024]{2,1,0:T(8,128)(2,1)} custom-call(s32[8]{0:T(128)S(1)} %copy-done.1, s32[2]{0:T(128)S(1)} %pad_add_fusion.1.side_ref, bf16[8,512,128]{2,1,0:T(8,128)(2,1)S(1)} %all_to_all.18.own_ref, bf16[8,512,128]{2,1,0:T(8,128)(2,1)} %collective-permute-done.2.other_ref, bf16[1024,1024]{1,0:T(8,128)(2,1)S(1)} %copy-done.2), custom_call_target="tpu_custom_call" | custom-call | flops 2147483648 | bytes 6291456 | tf_op jit(solution)/shard_map/output_projection/pallas_call | solution.py:423
  (5 shorter events, 0.0 us)
Async XLA Ops:
  6.3 6.2 %copy-start = (s32[8]{0:T(128)S(1)}, s32[8]{0:T(128)}, u32[]{:S(2)}) copy-start(s32[8]{0:T(128)} %lengths_ref.5) | copy-start | bytes 100
  6.3 21.3 %all-to-all-start = ((bf16[8,528,128]{2,1,0:T(8,128)(2,1)}), bf16[8,528,128]{2,1,0:T(8,128)(2,1)S(1)}, u32[]{:S(2)}, u32[]{:S(2)}) async-start(bf16[8,528,128]{2,1,0:T(8,128)(2,1)} %project.2), calls=%async_computation | async-start | bytes 2162688 | tf_op jit(solution)/shard_map/all_to_all | solution.py:463
  27.6 18.5 %all-to-all-start.1 = ((bf16[8,528,128]{2,1,0:T(8,128)(2,1)}), bf16[8,528,128]{2,1,0:T(8,128)(2,1)S(1)}, u32[]{:S(2)}, u32[]{:S(2)}) async-start(bf16[8,528,128]{2,1,0:T(8,128)(2,1)} %project.3), calls=%async_computation.1 | async-start | bytes 2162688 | tf_op jit(solution)/shard_map/all_to_all | solution.py:463
  31.2 15.7 %copy-start.1 = (s32[8]{0:T(128)S(1)}, s32[8]{0:T(128)}, u32[]{:S(2)}) copy-start(s32[8]{0:T(128)} %lengths_ref.5) | copy-start | bytes 100
  32.0 22.3 %collective-permute-start.1 = (bf16[8,128,128]{2,1,0:T(8,128)(2,1)S(1)}, bf16[8,128,128]{2,1,0:T(8,128)(2,1)S(1)}, u32[]{:S(2)}, u32[]{:S(2)}) collective-permute-start(bf16[8,128,128]{2,1,0:T(8,128)(2,1)S(1)} %slice.17), channel_id=1, source_target_pairs={{0,16},{2,18},{4,20},{6,22},{8,24},{10,26},{12,28},{14,30},{1,17},... | collective-permute-start | bytes 786440 | tf_op jit(solution)/shard_map/ppermute | solution.py:472
  58.6 21.4 %copy-start.2 = (bf16[1024,1024]{1,0:T(8,128)(2,1)S(1)}, bf16[1024,1024]{1,0:T(8,128)(2,1)}, u32[]{:S(2)}) copy-start(bf16[1024,1024]{1,0:T(8,128)(2,1)} %w_ref.1) | copy-start | bytes 6291460
  77.3 2.8 %collective-permute-start.2 = (bf16[8,512,128]{2,1,0:T(8,128)(2,1)S(1)}, bf16[8,512,128]{2,1,0:T(8,128)(2,1)}, u32[]{:S(2)}, u32[]{:S(2)}) collective-permute-start(bf16[8,512,128]{2,1,0:T(8,128)(2,1)S(1)} %all_to_all.18.own_ref), channel_id=1, source_target_pairs={{0,1},{1,0},{2,3},{3,2},{4,5},{5,4},{6,7},{7,6},{8,9},{9,8},{10,11... | collective-permute-start | bytes 3145736 | tf_op jit(solution)/shard_map/ppermute | solution.py:507

commit v5 on v4

--- a/solution.py
+++ b/solution.py
@@ -376,66 +376,94 @@
     )(lengths, where, lists, *operands)
 
 
-def output_kernel(
-    lengths_ref, side_ref, own_ref, other_ref, w_ref, out_ref,
-    order_ref, rows_buf, out_sems, *, planes, kv_local,
-):
-    seq_count, blk = out_ref.shape[0], out_ref.shape[1]
-    order_by_length(lengths_ref, order_ref, seq_count)
+def output_kernel(*refs, planes, kv_local, first):
+    if first:
+        side_ref, in_ref, w_ref, out_ref, w_next, w_buf, w_sem, next_sem = refs
+    else:
+        lengths_ref, side_ref, in_ref, w_ref, part_ref, out_ref = refs[:6]
+        out_sems, order_ref, rows_buf = refs[6:]
+        w_buf = w_ref
+    chunks, seq_rows = (out_ref if first else part_ref).shape[:2]
+    blk = seq_rows // 2
     half = kv_local * LANES
-    own_at = pl.multiple_of(side_ref[0] * half, half)
-    other_at = pl.multiple_of((1 - side_ref[0]) * half, half)
-
-    def rows(ref, rank):
+    if first:
+        own_at = pl.multiple_of(side_ref[0] * half, half)
+        other_at = pl.multiple_of((1 - side_ref[0]) * half, half)
+        load = pltpu.make_async_copy(w_ref.at[pl.ds(own_at, half)], w_buf, w_sem)
+        load.start()
+        ahead = pltpu.make_async_copy(w_ref.at[pl.ds(other_at, half)], w_next, next_sem)
+        ahead.start()
+    else:
+        order_by_length(lengths_ref, order_ref, 2 * chunks)
+
+    def rows(rank):
         p, j = place(rank, planes)
         return jnp.concatenate(
-            [ref[p * kv_local + h, j * blk:(j + 1) * blk, :] for h in range(kv_local)], axis=1
+            [in_ref[p * kv_local + h, j * blk:(j + 1) * blk, :] for h in range(kv_local)], axis=1
         )
 
     stores = []
-    for rank in range(0, seq_count, 2):
-        mine = jnp.concatenate([rows(own_ref, rank), rows(own_ref, rank + 1)], axis=0)
-        theirs = jnp.concatenate([rows(other_ref, rank), rows(other_ref, rank + 1)], axis=0)
-        o = jnp.dot(mine, w_ref[pl.ds(own_at, half), :], preferred_element_type=jnp.float32)
-        o = o + jnp.dot(
-            theirs, w_ref[pl.ds(other_at, half), :], preferred_element_type=jnp.float32
-        )
-        for r in (rank, rank + 1):
+    if first:
+        load.wait()
+        stores.append(ahead)
+    for i in range(chunks):
+        x = jnp.concatenate([rows(2 * i), rows(2 * i + 1)], axis=0)
+        o = jnp.dot(x, w_buf[...], preferred_element_type=jnp.float32)
+        if first:
+            out_ref[i] = o
+            continue
+        o = o + part_ref[i]
+        for r in (2 * i, 2 * i + 1):
             live = side_ref[1] < lengths_ref[order_ref[r]]
             rows_buf[r] = jnp.where(
-                live, o[(r - rank) * blk:(r - rank + 1) * blk], 0.0
+                live, o[(r - 2 * i) * blk:(r - 2 * i + 1) * blk], 0.0
             ).astype(jnp.bfloat16)
-            store = pltpu.make_async_copy(
-                rows_buf.at[r], out_ref.at[order_ref[r]], out_sems.at[r]
+            stores.append(
+                pltpu.make_async_copy(rows_buf.at[r], out_ref.at[order_ref[r]], out_sems.at[r])
             )
-            store.start()
-            stores.append(store)
+            stores[-1].start()
     for store in stores:
         store.wait()
 
 
-def output_projection(own, other, w_output, lengths, side, planes, kv_local, blk):
+def output_projection(x, part, w_output, lengths, side, planes, kv_local, blk):
     seq_count = lengths.shape[0]
     width = w_output.shape[1]
+    first = part is None
     smem = pl.BlockSpec(memory_space=pltpu.SMEM)
     vmem = pl.BlockSpec(memory_space=pltpu.VMEM)
     hbm = pl.BlockSpec(memory_space=HBM)
-    return pl.pallas_call(
-        functools.partial(output_kernel, planes=planes, kv_local=kv_local),
-        in_specs=[smem, smem, vmem, vmem, vmem],
-        out_specs=hbm,
-        out_shape=jax.ShapeDtypeStruct((seq_count, blk, width), jnp.bfloat16),
-        scratch_shapes=[
+    sums = (seq_count // 2, 2 * blk, width)
+    w_half = (kv_local * LANES, width)
+    if first:
+        w_output = pltpu.with_memory_space_constraint(w_output, HBM)
+        out_shape = [
+            jax.ShapeDtypeStruct(sums, jnp.float32), jax.ShapeDtypeStruct(w_half, jnp.bfloat16)
+        ]
+        specs, operands = [smem, vmem, hbm], (side, x, w_output)
+        scratch = [
+            pltpu.VMEM(w_half, jnp.bfloat16), pltpu.SemaphoreType.DMA, pltpu.SemaphoreType.DMA
+        ]
+    else:
+        out_shape = jax.ShapeDtypeStruct((seq_count, blk, width), jnp.bfloat16)
+        specs, operands = [smem, smem, vmem, vmem, vmem], (lengths, side, x, w_output, part)
+        scratch = [
+            pltpu.SemaphoreType.DMA((seq_count,)),
             pltpu.SMEM((seq_count,), jnp.int32),
             pltpu.VMEM((seq_count, blk, width), jnp.bfloat16),
-            pltpu.SemaphoreType.DMA((seq_count,)),
-        ],
+        ]
+    return pl.pallas_call(
+        functools.partial(output_kernel, planes=planes, kv_local=kv_local, first=first),
+        in_specs=specs,
+        out_specs=[vmem, pl.BlockSpec(memory_space=pl.ANY)] if first else hbm,
+        out_shape=out_shape,
+        scratch_shapes=scratch,
         compiler_params=pltpu.CompilerParams(vmem_limit_bytes=40 << 20),
         cost_estimate=pl.CostEstimate(
-            flops=2 * seq_count * blk * w_output.size, transcendentals=0, bytes_accessed=6 << 20
+            flops=2 * seq_count * blk * kv_local * LANES * width, transcendentals=0, bytes_accessed=6 << 20
         ),
-        name="output_projection",
-    )(lengths, side, own, other, w_output)
+        name="output_own" if first else "output_other",
+    )(*operands)
 
 
 def place(rank, planes):
@@ -506,7 +534,12 @@
     own = exchange(attended)
     other = lax.ppermute(own, "tp", [(0, 1), (1, 0)])
     side = jnp.stack([lax.axis_index("tp").astype(jnp.int32), here * blk])
-    return output_projection(own, other, w_output, lengths, side, planes, kv_local, blk)
+    finish = functools.partial(
+        output_projection, lengths=lengths, side=side, planes=planes,
+        kv_local=kv_local, blk=blk,
+    )
+    part, w_next = finish(own, None, w_output)
+    return finish(other, part, w_next)
 
 
 def fits(mesh, tokens, w_key, chosen):

time: 85 us -> 83.5 us (0.982)
  waiting for transfers between devices: 20.4 us -> 17.7 us
  Pallas kernels: 28.8 us -> 30.1 us
    ppermute x1, waiting for transfers between devices: 2.71 us -> 0.01 us  [per_device(): other = lax.ppermute(own, 'tp', [(0, 1), (1, 0)])]
    pallas_call x1 -> x2, Pallas kernels: 4.44 us -> 5.71 us  [output_projection(): pl.pallas_call(functools.partial(output_kernel, planes=planes, kv_local=k...]
  transfers between devices with their start and end apart: 4 -> 4, of which waited for: 3 -> 2; matrix products, arithmetic and copies ran while one was open for 2% -> 2% of each run, Pallas kernels for 16% -> 20%
where the time goes in v5:
time: 83.5 us; the launch traced here: 83.1 us
  Pallas kernels  30.1 us (36%)
  blocking collectives  18.5 us (22%)
  waiting for transfers between devices  17.7 us (21%)
  starting transfers between devices  14.3 us (17%)
  between operations  0.95 us (1%)
    all_to_all x1, blocking collectives, exchange(): lax.all_to_all(x, 'kv', split_axis=0, concat_axis=0, tiled=True, axis_ind...  18.5 us
    all_to_all x2, waiting for transfers between devices, exchange(): lax.all_to_all(x, 'kv', split_axis=0, concat_axis=0, tiled=True, axis_ind...  17.7 us
    pallas_call x2, Pallas kernels, project(): pl.pallas_call(functools.partial(project_kernel, ranks=ranks, slots=slots...  12.7 us
    pallas_call x2, Pallas kernels, attend(): pl.pallas_call(functools.partial(attend_kernel, early=early, split=split,...  11.7 us
    all_to_all x2, starting transfers between devices, exchange(): lax.all_to_all(x, 'kv', split_axis=0, concat_axis=0, tiled=True, axis_ind...  9.78 us
    pallas_call x2, Pallas kernels, output_projection(): pl.pallas_call(functools.partial(output_kernel, planes=planes, kv_local=k...  5.71 us
    ppermute x1, starting transfers between devices, to_second_half(): return lax.ppermute(x, 'kv', [(i, i + half) for i in range(half)])  4.51 us
  transfers between devices with their start and end apart: 4, of which 2 were waited for; matrix products, arithmetic and copies ran while one was open for 2% of the time, Pallas kernels for 20%

profile of v5, /device:TPU:0, one launch (start us, length us, event | category | flops | bytes accessed | tf_op | source)
XLA Modules:
  0.0 83.1 jit_solution(5373182486406877276)
XLA Ops:
  0.0 6.3 %project.2 = bf16[8,528,128]{2,1,0:T(8,128)(2,1)} custom-call(s32[8]{0:T(128)} %refs_0_.1, s32[8,1,32]{2,1,0:T(1,128)} %chosen_in.3, bf16[8,128,2048]{2,1,0:T(8,128)(2,1)} %tokens_ref.3, bf16[2048,512]{1,0:T(8,128)(2,1)} %wq_ref.3, bf16[2048,256]{1,0:T(8,128)(2,1)} %wk_ref.3, bf16[2048,256]{1,0:T(8,128)(2,1)} %wv_ref.3), custom_call_target="tpu_custom_call" | custom-call | flops 2147483648 | bytes 7372800 | tf_op jit(solution)/shard_map/project/pallas_call | solution.py:205
  6.3 0.0 copy-start
  6.3 6.2 %all-to-all-start = ((bf16[8,528,128]{2,1,0:T(8,128)(2,1)}), bf16[8,528,128]{2,1,0:T(8,128)(2,1)S(1)}, u32[]{:S(2)}, u32[]{:S(2)}) async-start(bf16[8,528,128]{2,1,0:T(8,128)(2,1)} %project.2), calls=%async_computation | async-start | bytes 2162688 | tf_op jit(solution)/shard_map/all_to_all | solution.py:491
  12.6 0.0 copy-done
  12.6 0.7 fusion
  13.2 6.3 %project.3 = bf16[8,528,128]{2,1,0:T(8,128)(2,1)} custom-call(s32[8]{0:T(128)} %refs_0_.1, s32[8,1,32]{2,1,0:T(1,128)} %chosen_in.3, bf16[8,128,2048]{2,1,0:T(8,128)(2,1)} %tokens_ref.3, bf16[2048,512]{1,0:T(8,128)(2,1)} %wq_ref.3, bf16[2048,256]{1,0:T(8,128)(2,1)} %wk_ref.3, bf16[2048,256]{1,0:T(8,128)(2,1)} %wv_ref.3), custom_call_target="tpu_custom_call" | custom-call | flops 2147483648 | bytes 7372800 | tf_op jit(solution)/shard_map/project/pallas_call | solution.py:205
  19.6 8.0 %all-to-all-done.refs_0_ = bf16[8,528,128]{2,1,0:T(8,128)(2,1)S(1)} async-done(((bf16[8,528,128]{2,1,0:T(8,128)(2,1)}), bf16[8,528,128]{2,1,0:T(8,128)(2,1)S(1)}, u32[]{:S(2)}, u32[]{:S(2)}) %all-to-all-start) | async-done | bytes 1081376 | tf_op jit(solution)/shard_map/all_to_all | solution.py:491
  27.6 3.6 %all-to-all-start.1 = ((bf16[8,528,128]{2,1,0:T(8,128)(2,1)}), bf16[8,528,128]{2,1,0:T(8,128)(2,1)S(1)}, u32[]{:S(2)}, u32[]{:S(2)}) async-start(bf16[8,528,128]{2,1,0:T(8,128)(2,1)} %project.3), calls=%async_computation.1 | async-start | bytes 2162688 | tf_op jit(solution)/shard_map/all_to_all | solution.py:491
  31.2 0.0 copy-start.1
  31.9 0.1 pad_add_fusion.2.where_ref
  32.0 4.5 %collective-permute-start.1 = (bf16[8,128,128]{2,1,0:T(8,128)(2,1)S(1)}, bf16[8,128,128]{2,1,0:T(8,128)(2,1)S(1)}, u32[]{:S(2)}, u32[]{:S(2)}) collective-permute-start(bf16[8,128,128]{2,1,0:T(8,128)(2,1)S(1)} %slice.17), channel_id=1, source_target_pairs={{0,16},{2,18},{4,20},{6,22},{8,24},{10,26},{12,28},{14,30},{1,17},... | collective-permute-start | bytes 786440 | tf_op jit(solution)/shard_map/ppermute | solution.py:500
  36.5 9.6 %all-to-all-done.1.refs_1_ = bf16[8,528,128]{2,1,0:T(8,128)(2,1)S(1)} async-done(((bf16[8,528,128]{2,1,0:T(8,128)(2,1)}), bf16[8,528,128]{2,1,0:T(8,128)(2,1)S(1)}, u32[]{:S(2)}, u32[]{:S(2)}) %all-to-all-start.1) | async-done | bytes 1081376 | tf_op jit(solution)/shard_map/all_to_all | solution.py:491
  46.1 0.7 conditional.1
  46.1 0.7 broadcast.7
  46.9 0.0 copy-done.1
  46.9 7.4 %attend_early.1.refs_4_ = bf16[8,512,128]{2,1,0:T(8,128)(2,1)S(1)} custom-call(s32[8]{0:T(128)S(1)} %copy-done.1, s32[2]{0:T(128)S(1)} %pad_add_fusion.2.where_ref, s32[2048]{0:T(1024)S(1)} %bitcast.6, bf16[8,528,128]{2,1,0:T(8,128)(2,1)S(1)} %all-to-all-done.refs_0_), custom_call_target="tpu_custom_call" | custom-call | flops 2147483648 | bytes 3145728 | tf_op jit(solution)/shard_map/attend_early/pallas_call | solution.py:353
  54.2 0.0 collective-permute-done.1.refs_2_
  54.3 4.3 %attend.1 = bf16[8,512,128]{2,1,0:T(8,128)(2,1)S(1)} custom-call(s32[8]{0:T(128)S(1)} %copy-done.1, s32[2]{0:T(128)S(1)} %pad_add_fusion.2.where_ref, s32[4096]{0:T(1024)S(1)} %bitcast.7, bf16[8,528,128]{2,1,0:T(8,128)(2,1)S(1)} %all-to-all-done.refs_0_, bf16[8,528,128]{2,1,0:T(8,128)(2,1)S(1)} %all-to-all-done.1.refs_1_, ...), custom_call_target="tpu_custom_call", output_to_operand_aliasing={{}: (7, {})} | custom-call | flops 2147483648 | bytes 3145728 | tf_op jit(solution)/shard_map/attend/pallas_call | solution.py:353
  58.6 18.5 %all_to_all.18.refs_1_ = bf16[8,512,128]{2,1,0:T(8,128)(2,1)S(1)} all-to-all(bf16[8,512,128]{2,1,0:T(8,128)(2,1)S(1)} %attend.1), channel_id=1, replica_groups={{0,2,4,6,8,10,12,14},{16,18,20,22,24,26,28,30},{1,3,5,7,9,11,13,15},{17..., dimensions={0} | all-to-all | bytes 2097152 | tf_op jit(solution)/shard_map/all_to_all | solution.py:491
  77.1 0.0 collective-permute-start.2
  77.1 0.1 pad_add_fusion.1.refs_0_.refs_1_
  77.2 3.1 %output_own.1 = (f32[4,256,1024]{2,1,0:T(8,128)S(1)}, bf16[512,1024]{1,0:T(8,128)(2,1)S(1)}) custom-call(s32[2]{0:T(128)S(1)} %pad_add_fusion.1.refs_0_.refs_1_, bf16[8,512,128]{2,1,0:T(8,128)(2,1)S(1)} %all_to_all.18.refs_1_, bf16[1024,1024]{1,0:T(8,128)(2,1)} %refs_2_.1), custom_call_target="tpu_custom_call" | custom-call | flops 1073741824 | bytes 6291456 | tf_op jit(solution)/shard_map/output_own/pallas_call | solution.py:455
  80.3 0.0 collective-permute-done.2.refs_2_
  80.3 2.6 %output_other.1 = bf16[8,128,1024]{2,1,0:T(8,128)(2,1)} custom-call(s32[8]{0:T(128)S(1)} %copy-done.1, s32[2]{0:T(128)S(1)} %pad_add_fusion.1.refs_0_.refs_1_, bf16[8,512,128]{2,1,0:T(8,128)(2,1)S(1)} %collective-permute-done.2.refs_2_, bf16[512,1024]{1,0:T(8,128)(2,1)S(1)} %get-tuple-element.17.refs_3_, f32[4,256,1024]{2,1,0:T(8,128)S(1)} %get-tuple-element.18.refs_4_), custom_call_target="tpu_custom_call" | custom-call | flops 1073741824 | bytes 6291456 | tf_op jit(solution)/shard_map/output_other/pallas_call | solution.py:455
  (4 shorter events, 0.0 us)
Async XLA Ops:
  6.3 6.2 %copy-start = (s32[8]{0:T(128)S(1)}, s32[8]{0:T(128)}, u32[]{:S(2)}) copy-start(s32[8]{0:T(128)} %refs_0_.1) | copy-start | bytes 100
  6.3 21.3 %all-to-all-start = ((bf16[8,528,128]{2,1,0:T(8,128)(2,1)}), bf16[8,528,128]{2,1,0:T(8,128)(2,1)S(1)}, u32[]{:S(2)}, u32[]{:S(2)}) async-start(bf16[8,528,128]{2,1,0:T(8,128)(2,1)} %project.2), calls=%async_computation | async-start | bytes 2162688 | tf_op jit(solution)/shard_map/all_to_all | solution.py:491
  27.6 18.5 %all-to-all-start.1 = ((bf16[8,528,128]{2,1,0:T(8,128)(2,1)}), bf16[8,528,128]{2,1,0:T(8,128)(2,1)S(1)}, u32[]{:S(2)}, u32[]{:S(2)}) async-start(bf16[8,528,128]{2,1,0:T(8,128)(2,1)} %project.3), calls=%async_computation.1 | async-start | bytes 2162688 | tf_op jit(solution)/shard_map/all_to_all | solution.py:491
  31.2 15.7 %copy-start.1 = (s32[8]{0:T(128)S(1)}, s32[8]{0:T(128)}, u32[]{:S(2)}) copy-start(s32[8]{0:T(128)} %refs_0_.1) | copy-start | bytes 100
  32.0 22.3 %collective-permute-start.1 = (bf16[8,128,128]{2,1,0:T(8,128)(2,1)S(1)}, bf16[8,128,128]{2,1,0:T(8,128)(2,1)S(1)}, u32[]{:S(2)}, u32[]{:S(2)}) collective-permute-start(bf16[8,128,128]{2,1,0:T(8,128)(2,1)S(1)} %slice.17), channel_id=1, source_target_pairs={{0,16},{2,18},{4,20},{6,22},{8,24},{10,26},{12,28},{14,30},{1,17},... | collective-permute-start | bytes 786440 | tf_op jit(solution)/shard_map/ppermute | solution.py:500
  77.1 3.2 %collective-permute-start.2 = (bf16[8,512,128]{2,1,0:T(8,128)(2,1)S(1)}, bf16[8,512,128]{2,1,0:T(8,128)(2,1)S(1)}, u32[]{:S(2)}, u32[]{:S(2)}) collective-permute-start(bf16[8,512,128]{2,1,0:T(8,128)(2,1)S(1)} %all_to_all.18.refs_1_), channel_id=1, source_target_pairs={{0,1},{1,0},{2,3},{3,2},{4,5},{5,4},{6,7},{7,6},{8,9},{9,8},{10,11... | collective-permute-start | bytes 3145736 | tf_op jit(solution)/shard_map/ppermute | solution.py:535
